TPU v7x, 32 devices: a whole 2x2x4 slice. The times are simulated.
32 devices in a mesh: ep: 16 (over z, y, x), tp: 2 (over core).
Axes of the slice: x: 2, y: 2, z: 4, core: 2. Of those that a mesh axis runs over, the one named last changes fastest.
Arguments:
- inputs: bfloat16 [8192, 2048], P(('ep', 'tp')), may hold values from -6 to 6
- pre_gain: float32 [2048], replicated, may hold values from 0.5 to 8
- expert_ids: int32 [8192, 2], P(('ep', 'tp')), may hold values from 0 to 15, all different within a row; in each aligned block of 256 rows (0 to 255, 256 to 511, ...) at most 48 rows name the same one
- route_weights: float32 [8192, 2], P(('ep', 'tp')), may hold values from 0.05 to 1
- gate_proj: bfloat16 [16, 2048, 2048], P('ep', None, 'tp'), may hold values from -0.125 to 0.125
- up_proj: bfloat16 [16, 2048, 2048], P('ep', None, 'tp'), may hold values from -0.125 to 0.125
- down_proj: bfloat16 [16, 2048, 2048], P('ep', 'tp'), may hold values from -0.125 to 0.125
- post_gain: float32 [2048], replicated, may hold values from 0.1 to 1.9
Outputs:
- layer_out: bfloat16 [8192, 2048], P(('ep', 'tp'))
Inputs may be any that keep to these rules, and one draw needn't show every extreme that they name: `expert_ids`: each token names 2 different experts. Among the 256 tokens of one device (aligned blocks of rows) no expert is named by more than 48 tokens, and in every draw some expert is named by exactly 48 tokens of some device.
All inputs are finite; a program needn't handle non-finite values.
Results may differ from a plain program's by a relative error of at most 0.0095.
Values may be sent and summed in bfloat16 or wider, within the bound.
A program may use at most 128 MiB of HBM per device.

v0:
```python
import functools

import jax
import jax.numpy as jnp
from jax import lax
from jax.experimental import pallas as pl
from jax.experimental.pallas import tpu as pltpu
from jax.sharding import PartitionSpec as P

EPSILON = 1e-06
LIMIT = 7.0
ALPHA = 1.702
CHUNKS = 4
TILE = 256
MESH = pl.DeviceIdType.MESH


def activate(gate, up):
    gate = jnp.minimum(gate, LIMIT)
    up = jnp.clip(up, -LIMIT, LIMIT)
    return ((up + 1.0) * gate * jax.nn.sigmoid(ALPHA * gate)).astype(jnp.bfloat16)


def dot(a, b):
    return jnp.dot(a, b, preferred_element_type=jnp.float32)


def kernel(
    n, tps, cap,
    x_ref, pre_ref, meta_ref, gate_ref, up_ref, down_ref, post_ref, out_ref,
    gate_v, up_v, down_v, normed, prox, pmeta, send, recv, ret, acc, part_send, part_recv,
    mixed, hidden, places,
    w_local, w_send, w_recv, p_send, p_recv, m_send, m_recv,
    d_send, d_recv, r_send, r_recv, q_send, q_recv,
):
    half = n // 2
    tokens, width = x_ref.shape
    cw = width // CHUNKS
    rows = half * cap
    fh = gate_v.shape[2]
    me = lax.axis_index("ep")
    core = lax.axis_index("tp")
    base = (me // half) * half
    mine = lax.rem(me, half)
    proxy = lax.rem(me + half, n)

    def member(j):
        return base + lax.rem(mine + j, half)

    barrier = pltpu.get_barrier_semaphore()

    @pl.loop(1, half)
    def _(j):
        pl.semaphore_signal(barrier, inc=1, device_id={"ep": member(j)}, device_id_type=MESH)

    pl.semaphore_signal(barrier, inc=1, device_id={"ep": proxy}, device_id_type=MESH)
    for i in range(1, tps):
        pl.semaphore_signal(
            barrier, inc=1, device_id={"tp": lax.rem(core + i, tps)}, device_id_type=MESH
        )
    pl.semaphore_wait(barrier, half + tps - 1)

    def remote(src, dst, ss, rs, where):
        return pltpu.make_async_remote_copy(
            src_ref=src, dst_ref=dst, send_sem=ss, recv_sem=rs,
            device_id=where, device_id_type=MESH,
        )

    def await_bytes(ref, sem):
        pltpu.make_async_copy(ref, ref, sem).wait()

    remote(meta_ref, pmeta, m_send, m_recv, {"ep": proxy}).start()
    weights = ((gate_ref, gate_v), (up_ref, up_v), (down_ref, down_v))
    local_copies, peer_copies = [], []
    for w, (src, dst) in enumerate(weights):
        local_copies.append(pltpu.make_async_copy(src.at[0], dst.at[core], w_local.at[w]))
        for i in range(1, tps):
            peer_copies.append(
                remote(
                    src.at[0], dst.at[core], w_send.at[w, i - 1], w_recv.at[w, i - 1],
                    {"tp": lax.rem(core + i, tps)},
                )
            )
    for copy in peer_copies + local_copies:
        copy.start()

    experts_col = lax.broadcasted_iota(jnp.int32, (n, 1), 0).astype(jnp.float32)
    earlier_mask = (
        lax.broadcasted_iota(jnp.int32, (tokens, tokens), 0)
        < lax.broadcasted_iota(jnp.int32, (tokens, tokens), 1)
    ).astype(jnp.bfloat16)

    def place(k, meta):
        first, second = meta[0:1, :], meta[1:2, :]
        hot0 = (first == experts_col).astype(jnp.float32)
        hot1 = (second == experts_col).astype(jnp.float32)
        before = dot((hot0 + hot1).astype(jnp.bfloat16), earlier_mask)
        places[k] = meta
        for i, (ids, hot) in enumerate(((first, hot0), (second, hot1))):
            slot = jnp.sum(before * hot, axis=0, keepdims=True)
            relative = ids - (base + mine).astype(jnp.float32)
            inside = (ids >= base.astype(jnp.float32)) & (
                ids < (base + half).astype(jnp.float32)
            )
            relative = jnp.where(relative < 0, relative + half, relative)
            places[k, i : i + 1, :] = jnp.where(inside, relative * cap + slot, -1.0)

    def picker(k):
        at = lax.broadcasted_iota(jnp.int32, (rows, 1), 0).astype(jnp.float32)
        return (
            (places[k, 0:1, :] == at).astype(jnp.float32)
            + (places[k, 1:2, :] == at).astype(jnp.float32)
        ).astype(jnp.bfloat16)

    def mixer(k):
        columns = places[k].T
        at = lax.broadcasted_iota(jnp.int32, (1, rows), 1).astype(jnp.float32)
        w = jnp.where(columns[:, 0:1] == at, columns[:, 2:3], 0.0) + jnp.where(
            columns[:, 1:2] == at, columns[:, 3:4], 0.0
        )
        high = w.astype(jnp.bfloat16)
        return high, (w - high.astype(jnp.float32)).astype(jnp.bfloat16)

    def dispatch(k, c, values):
        picked = dot(picker(k), values).astype(jnp.bfloat16)
        recv[k, c, 0:cap, :] = picked[0:cap]
        send[k, c, cap:rows, :] = picked[cap:rows]

        @pl.loop(1, half)
        def _(j):
            block = pl.ds(pl.multiple_of(j * cap, cap), cap)
            remote(
                send.at[k, c, block], recv.at[k, c, block], d_send.at[k, c], d_recv.at[k, c],
                {"ep": member(j)},
            ).start()

    def give_back(k, c):
        @pl.loop(1, half)
        def _(j):
            block = pl.ds(pl.multiple_of(j * cap, cap), cap)
            remote(
                send.at[k, c, block], ret.at[k, c, block], r_send.at[k, c], r_recv.at[k, c],
                {"ep": member(half - j)},
            ).start()

    squares = jnp.zeros((tokens, 1), jnp.float32)
    for c in range(CHUNKS):
        xs = x_ref[:, c * cw : (c + 1) * cw].astype(jnp.float32)
        squares = squares + jnp.sum(xs * xs, axis=-1, keepdims=True)
    scale = lax.rsqrt(squares / width + EPSILON)
    proxied = [
        remote(normed.at[c], prox.at[c], p_send.at[c], p_recv.at[c], {"ep": proxy})
        for c in range(CHUNKS)
    ]

    def normalise(c):
        xs = x_ref[:, c * cw : (c + 1) * cw].astype(jnp.float32)
        normed[c] = (xs * scale * pre_ref[:, c * cw : (c + 1) * cw]).astype(jnp.bfloat16)

    def own(c):
        dispatch(0, c, normed[c])

    def relay(c):
        proxied[c].wait_recv()
        dispatch(1, c, prox[c])

    meta_copy = remote(meta_ref, pmeta, m_send, m_recv, {"ep": proxy})
    normalise(0)
    proxied[0].start()
    place(0, meta_ref[...])
    own(0)
    normalise(1)
    proxied[1].start()
    own(1)
    normalise(2)
    normalise(3)
    meta_copy.wait_recv()
    place(1, pmeta[...])

    def received(k, c):
        await_bytes(recv.at[k, c, pl.ds(cap, rows - cap)], d_recv.at[k, c])

    def expand(k, halves, chunks, begin=True, end=True, tiles=(0, fh // TILE)):
        for h in halves:
            @pl.loop(*tiles)
            def _(t):
                at = pl.ds(pl.multiple_of(t * TILE, TILE), TILE)
                if begin:
                    gate = jnp.zeros((rows, TILE), jnp.float32)
                    up = jnp.zeros((rows, TILE), jnp.float32)
                else:
                    gate = acc[0, h, :, at]
                    up = acc[1, h, :, at]
                for c in chunks:
                    gate += dot(recv[k, c], gate_v[h, c * cw : (c + 1) * cw, at])
                    up += dot(recv[k, c], up_v[h, c * cw : (c + 1) * cw, at])
                if end:
                    hidden[k, h, :, at] = activate(gate, up)
                else:
                    acc[0, h, :, at] = gate
                    acc[1, h, :, at] = up

    def contract(k, c):
        await_bytes(send.at[k, c, pl.ds(cap, rows - cap)], d_send.at[k, c])
        for t in range(cw // TILE):
            lo = t * TILE
            total = jnp.zeros((rows, TILE), jnp.float32)
            for h in range(tps):
                at = pl.ds(pl.multiple_of(c * cw + lo, TILE), TILE)
                total += dot(hidden[k, h], down_v[h, :, at]).astype(jnp.bfloat16).astype(jnp.float32)
            total = total.astype(jnp.bfloat16)
            ret[k, c, 0:cap, lo : lo + TILE] = total[0:cap]
            send[k, c, cap:rows, lo : lo + TILE] = total[cap:rows]
        give_back(k, c)

    both = range(tps)
    last = fh // TILE
    relay(0)
    proxied[2].start()
    for copy in local_copies:
        copy.wait()
    for copy in peer_copies:
        copy.wait()
    relay(1)
    proxied[3].start()
    received(1, 0)
    received(1, 1)
    expand(1, both, (0, 1), end=False)
    relay(2)
    received(1, 2)
    expand(1, both, (2,), begin=False, end=False)
    relay(3)
    own(2)
    own(3)
    received(1, 3)
    expand(1, both, (3,), begin=False)

    shares = []
    high1, low1 = mixer(1)

    def share(c):
        await_bytes(ret.at[1, c, pl.ds(cap, rows - cap)], r_recv.at[1, c])
        part_send[c] = (dot(high1, ret[1, c]) + dot(low1, ret[1, c])).astype(jnp.bfloat16)
        copy = remote(part_send.at[c], part_recv.at[c], q_send.at[c], q_recv.at[c], {"ep": proxy})
        copy.start()
        shares.append(copy)

    contract(1, 0)
    contract(1, 1)
    for c in range(CHUNKS):
        received(0, c)
    every = range(CHUNKS)
    expand(0, (0,), every, tiles=(0, last // 2))
    share(0)
    contract(1, 2)
    expand(0, (0,), every, tiles=(last // 2, last))
    share(1)
    contract(1, 3)
    expand(0, range(1, tps), every, tiles=(0, last // 2))
    share(2)
    expand(0, range(1, tps), every, tiles=(last // 2, last))
    share(3)

    @pl.loop(0, CHUNKS)
    def _(c):
        contract(0, c)

    high0, low0 = mixer(0)
    for c in range(CHUNKS):
        await_bytes(ret.at[0, c, pl.ds(cap, rows - cap)], r_recv.at[0, c])
        mixed[c] = dot(high0, ret[0, c]) + dot(low0, ret[0, c])

    squares = jnp.zeros((tokens, 1), jnp.float32)
    for c in range(CHUNKS):
        shares[c].wait_recv()
        total = mixed[c] + part_recv[c].astype(jnp.float32)
        mixed[c] = total
        squares = squares + jnp.sum(total * total, axis=-1, keepdims=True)
    scale = lax.rsqrt(squares / width + EPSILON)
    for c in range(CHUNKS):
        at = slice(c * cw, (c + 1) * cw)
        out_ref[:, at] = (mixed[c] * scale * post_ref[:, at]).astype(jnp.bfloat16)

    meta_copy.wait_send()
    for c in range(CHUNKS):
        proxied[c].wait_send()
        shares[c].wait_send()
        for k in range(2):
            await_bytes(send.at[k, c, pl.ds(cap, rows - cap)], r_send.at[k, c])


def local(inputs, pre_gain, expert_ids, route_weights, gate_proj, up_proj, down_proj, post_gain):
    tokens, width = inputs.shape
    choices = expert_ids.shape[1]
    n = lax.axis_size("ep")
    tps = lax.axis_size("tp")
    cap = 3 * tokens * choices // (2 * n * gate_proj.shape[0])
    cap = -(-cap // 16) * 16
    half = n // 2
    rows = half * cap
    cw = width // CHUNKS
    fh = gate_proj.shape[2]
    meta = jnp.concatenate(
        [
            expert_ids.astype(jnp.float32),
            route_weights,
            jnp.zeros((tokens, 8 - 2 * choices), jnp.float32),
        ],
        axis=1,
    ).T
    bf16 = jnp.bfloat16
    vmem = pl.BlockSpec(memory_space=pltpu.VMEM)
    hbm = pl.BlockSpec(memory_space=pl.ANY)
    dma = pltpu.SemaphoreType.DMA
    return pl.pallas_call(
        functools.partial(kernel, n, tps, cap),
        out_shape=jax.ShapeDtypeStruct((tokens, width), bf16),
        in_specs=[vmem, vmem, vmem, hbm, hbm, hbm, vmem],
        out_specs=vmem,
        scratch_shapes=[
            pltpu.VMEM((tps, width, fh), bf16),
            pltpu.VMEM((tps, width, fh), bf16),
            pltpu.VMEM((tps, fh, width), bf16),
            pltpu.VMEM((CHUNKS, tokens, cw), bf16),
            pltpu.VMEM((CHUNKS, tokens, cw), bf16),
            pltpu.VMEM((8, tokens), jnp.float32),
            pltpu.VMEM((2, CHUNKS, rows, cw), bf16),
            pltpu.VMEM((2, CHUNKS, rows, cw), bf16),
            pltpu.VMEM((2, CHUNKS, rows, cw), bf16),
            pltpu.VMEM((2, tps, rows, fh), jnp.float32),
            pltpu.VMEM((CHUNKS, tokens, cw), bf16),
            pltpu.VMEM((CHUNKS, tokens, cw), bf16),
            pltpu.VMEM((CHUNKS, tokens, cw), jnp.float32),
            pltpu.VMEM((2, tps, rows, fh), bf16),
            pltpu.VMEM((2, 8, tokens), jnp.float32),
            dma((3,)), dma((3, tps - 1)), dma((3, tps - 1)),
            dma((CHUNKS,)), dma((CHUNKS,)), dma, dma,
            dma((2, CHUNKS)), dma((2, CHUNKS)), dma((2, CHUNKS)), dma((2, CHUNKS)),
            dma((CHUNKS,)), dma((CHUNKS,)),
        ],
        compiler_params=pltpu.CompilerParams(
            collective_id=0, has_side_effects=True, vmem_limit_bytes=67043328
        ),
    )(inputs, pre_gain[None, :], meta, gate_proj, up_proj, down_proj, post_gain[None, :])


def solution(mesh):
    in_specs = (
        P(("ep", "tp"), None),
        P(),
        P(("ep", "tp"), None),
        P(("ep", "tp"), None),
        P("ep", None, "tp"),
        P("ep", None, "tp"),
        P("ep", "tp", None),
        P(),
    )
    out_specs = P(("ep", "tp"), None)
    return jax.shard_map(local, mesh=mesh, in_specs=in_specs, out_specs=out_specs, check_vma=False)
```

profile of v0, /device:TPU:0, one launch (start us, length us, event | category | flops | bytes accessed | tf_op | source)
XLA Modules:
  0.0 143.0 jit_solution(14910470003516384915)
XLA Ops:
  0.0 0.1 pad.2.clone
  0.1 0.7 convert_element_type.3
  0.8 1.3 maximum_bitcast_fusion.meta_ref
  2.1 138.6 %shard_map.82 = bf16[256,2048]{1,0:T(8,128)(2,1)} custom-call(bf16[256,2048]{1,0:T(8,128)(2,1)} %x_ref.1, f32[1,2048]{1,0:T(1,128)} %bitcast.4, f32[8,256]{1,0:T(8,128)} %maximum_bitcast_fusion.meta_ref, bf16[1,2048,1024]{2,1,0:T(8,128)(2,1)} %gate_ref.1, bf16[1,2048,1024]{2,1,0:T(8,128)(2,1)} %up_ref.1, bf16[1,1024,2048]{2,1,0:T(8,128)(2,1)} %down_ref.1, ...), custom_call_target="tpu_custom_call" | custom-call | tf_op jit(solution)/shard_map/pallas_call | solution.py:315
  140.7 2.3 %copy.10 = bf16[256,2048]{1,0:T(8,128)(2,1)} copy(bf16[256,2048]{1,0:T(8,128)(2,1)} %shard_map.82) | data formatting | bytes 2097152
  (1 shorter events, 0.0 us)
where the time goes:
time: 143 us
  Pallas kernels  139 us (97%)
  local copies, waits for them, and re-layouts  2.38 us (2%)
  other arithmetic  2.03 us (1%)
    pallas_call x1, Pallas kernels, local(): pl.pallas_call(functools.partial(kernel, n, tps, cap), out_shape=jax.Shap...  139 us

commit v1 on v0

v1 whole, which is shorter than its diff:
```python
import functools

import jax
import jax.numpy as jnp
from jax import lax
from jax.experimental import pallas as pl
from jax.experimental.pallas import tpu as pltpu
from jax.sharding import PartitionSpec as P

EPSILON = 1e-06
LIMIT = 7.0
ALPHA = 1.702
CHUNKS = 4
TILE = 256
PLANES = 4
MESH = pl.DeviceIdType.MESH


def activate(gate, up):
    gate = jnp.minimum(gate, LIMIT)
    up = jnp.clip(up, -LIMIT, LIMIT)
    return ((up + 1.0) * gate * jax.nn.sigmoid(ALPHA * gate)).astype(jnp.bfloat16)


def dot(a, b):
    return jnp.dot(a, b, preferred_element_type=jnp.float32)


def kernel(
    n, tps, cap,
    x_hbm, pre_ref, ids_ref, route_ref, gate_ref, up_ref, down_ref, post_ref, out_ref,
    x_ref, gate_v, up_v, down_v, held, meta, send, recv, ret,
    fp_send, fp_recv, mixed, hidden, places,
    x_sem, w_local, w_send, w_recv, n_send, n_recv, m_send, m_recv,
    d_send, d_recv, r_send, r_recv, q_send, q_recv,
):
    tokens, width = x_ref.shape
    pz = n // PLANES
    cw = width // CHUNKS
    rows = pz * cap
    fh = gate_v.shape[2]
    every = range(CHUNKS)
    me = lax.axis_index("ep")
    core = lax.axis_index("tp")
    plane = me // pz
    column = lax.rem(me, pz)
    inner = plane * (3 - plane) // 2
    outer = 1 - inner
    mine = outer
    mate_base = (plane + 1 - 2 * lax.rem(plane, 2)) * pz
    own_base = plane * pz
    mate = mate_base + column
    far = (3 - plane) * pz + column

    def on_inner(f):
        pl.when(inner == 1)(f)

    def on_outer(f):
        pl.when(inner == 0)(f)

    def ring(base, j):
        return base + lax.rem(column + j, pz)

    def greet(device):
        pl.semaphore_signal(barrier, inc=1, device_id=device, device_id_type=MESH)

    x_copy = pltpu.make_async_copy(x_hbm, x_ref, x_sem)
    x_copy.start()
    weights = ((gate_ref, gate_v), (up_ref, up_v), (down_ref, down_v))
    local_copies = [
        pltpu.make_async_copy(src.at[0], dst.at[core], w_local.at[w])
        for w, (src, dst) in enumerate(weights)
    ]
    for copy in local_copies:
        copy.start()

    barrier = pltpu.get_barrier_semaphore()

    @pl.loop(1, pz)
    def _(j):
        greet({"ep": ring(own_base, j)})

    @pl.loop(0, pz)
    def _(j):
        greet({"ep": ring(mate_base, j)})

    for i in range(1, tps):
        greet({"tp": lax.rem(core + i, tps)})

    @on_inner
    def _():
        greet({"ep": far})

    pl.semaphore_wait(barrier, 2 * pz - 1 + tps - 1 + inner)

    def remote(src, dst, ss, rs, where):
        return pltpu.make_async_remote_copy(
            src_ref=src, dst_ref=dst, send_sem=ss, recv_sem=rs,
            device_id=where, device_id_type=MESH,
        )

    def await_bytes(ref, sem):
        pltpu.make_async_copy(ref, ref, sem).wait()

    peer_copies = [
        [
            remote(
                src.at[0], dst.at[core], w_send.at[w, i - 1], w_recv.at[w, i - 1],
                {"tp": lax.rem(core + i, tps)},
            )
            for i in range(1, tps)
        ]
        for w, (src, dst) in enumerate(weights)
    ]
    for copies in peer_copies:
        for copy in copies:
            copy.start()

    meta[mine, 0:2, :] = ids_ref[...].astype(jnp.float32)
    meta[mine, 2:4, :] = route_ref[...]
    meta[mine, 4:8, :] = jnp.zeros((4, tokens), jnp.float32)

    def place(g, ts):
        values = meta[g]
        experts_col = lax.broadcasted_iota(jnp.int32, (n, 1), 0).astype(jnp.float32)
        earlier = (
            lax.broadcasted_iota(jnp.int32, (tokens, tokens), 0)
            < lax.broadcasted_iota(jnp.int32, (tokens, tokens), 1)
        ).astype(jnp.bfloat16)
        first, second = values[0:1, :], values[1:2, :]
        hot0 = (first == experts_col).astype(jnp.float32)
        hot1 = (second == experts_col).astype(jnp.float32)
        before = dot((hot0 + hot1).astype(jnp.bfloat16), earlier)
        for t in ts:
            start = (mate_base if t else own_base).astype(jnp.float32)
            places[2 * g + t] = values
            for i, (ids, hot) in enumerate(((first, hot0), (second, hot1))):
                slot = jnp.sum(before * hot, axis=0, keepdims=True)
                inside = (ids >= start) & (ids < start + pz)
                relative = ids - (start + column.astype(jnp.float32))
                relative = jnp.where(relative < 0, relative + pz, relative)
                places[2 * g + t, i : i + 1, :] = jnp.where(inside, relative * cap + slot, -1.0)

    def picker(k):
        at = lax.broadcasted_iota(jnp.int32, (rows, 1), 0).astype(jnp.float32)
        return (
            (places[k, 0:1, :] == at).astype(jnp.float32)
            + (places[k, 1:2, :] == at).astype(jnp.float32)
        ).astype(jnp.bfloat16)

    def mixer(k):
        columns = places[k].T
        at = lax.broadcasted_iota(jnp.int32, (1, rows), 1).astype(jnp.float32)
        w = jnp.where(columns[:, 0:1] == at, columns[:, 2:3], 0.0) + jnp.where(
            columns[:, 1:2] == at, columns[:, 3:4], 0.0
        )
        high = w.astype(jnp.bfloat16)
        return high, (w - high.astype(jnp.float32)).astype(jnp.bfloat16)

    def block_of(j):
        return pl.ds(pl.multiple_of(j * cap, cap), cap)

    def pick(g, t, c):
        k = 2 * g + t
        picked = dot(picker(k), held[g, c]).astype(jnp.bfloat16)
        if t == 0:
            recv[g, c, 0:cap, :] = picked[0:cap]
            send[k, c, cap:rows, :] = picked[cap:rows]
        else:
            send[k, c] = picked
        base = mate_base if t else own_base

        @pl.loop(1 - t, pz)
        def _(j):
            remote(
                send.at[k, c, block_of(j)], recv.at[g, c, block_of(j)],
                d_send.at[k, c], d_recv.at[g, c], {"ep": ring(base, j)},
            ).start()

    def received_in_plane(g):
        @pl.loop(0, CHUNKS)
        def _(c):
            await_bytes(recv.at[g, c, pl.ds(cap, rows - cap)], d_recv.at[g, c])

    def received_crossed(g):
        @pl.loop(0, CHUNKS)
        def _(c):
            await_bytes(recv.at[g, c], d_recv.at[g, c])

    def received(g):
        on_inner(lambda: received_in_plane(g))
        on_outer(lambda: received_crossed(g))

    def expand(g, i):
        h = lax.rem(core + i, tps)

        @pl.loop(0, fh // TILE)
        def _(t):
            at = pl.ds(pl.multiple_of(t * TILE, TILE), TILE)
            gate = jnp.zeros((rows, TILE), jnp.float32)
            up = jnp.zeros((rows, TILE), jnp.float32)
            for c in every:
                gate += dot(recv[g, c], gate_v[h, c * cw : (c + 1) * cw, at])
                up += dot(recv[g, c], up_v[h, c * cw : (c + 1) * cw, at])
            hidden[g, h, :, at] = activate(gate, up)

    def contract(g, t):
        k = 2 * g + t
        base = own_base + t * (mate_base - own_base)

        @pl.loop(0, CHUNKS)
        def _(c):
            for s in range(cw // TILE):
                lo = s * TILE
                total = jnp.zeros((rows, TILE), jnp.float32)
                for h in range(tps):
                    at = pl.ds(pl.multiple_of(c * cw + lo, TILE), TILE)
                    part = dot(hidden[g, h], down_v[h, :, at])
                    total += part.astype(jnp.bfloat16).astype(jnp.float32)
                recv[g, c, :, lo : lo + TILE] = total.astype(jnp.bfloat16)

            @pl.when(t == 0)
            def _():
                ret[k, c, 0:cap, :] = recv[g, c, 0:cap, :]

            @pl.loop(1 - t, pz)
            def _(j):
                remote(
                    recv.at[g, c, block_of(j)], ret.at[k, c, block_of(j)],
                    r_send.at[g, c], r_recv.at[k, c], {"ep": ring(base, pz - j)},
                ).start()

    def mix(g, t, c):
        k = 2 * g + t
        high, low = mixer(k)
        if t == 0:
            await_bytes(ret.at[k, c, pl.ds(cap, rows - cap)], r_recv.at[k, c])
        else:
            await_bytes(ret.at[k, c], r_recv.at[k, c])
        return dot(high, ret[k, c]) + dot(low, ret[k, c])

    x_copy.wait()
    squares = jnp.zeros((tokens, 1), jnp.float32)
    for c in every:
        xs = x_ref[:, c * cw : (c + 1) * cw].astype(jnp.float32)
        squares = squares + jnp.sum(xs * xs, axis=-1, keepdims=True)
    scale = lax.rsqrt(squares / width + EPSILON)
    partner = far * inner + mate * outer

    def rows_copy(step, c):
        if step == 0:
            return remote(
                held.at[mine, c], held.at[1 + inner, c], n_send.at[0, c], n_recv.at[1 + inner, c],
                {"ep": partner},
            )
        return remote(
            held.at[1, c], held.at[3, c], n_send.at[1, c], n_recv.at[3, c], {"ep": far}
        )

    def meta_copy(step):
        if step == 0:
            return remote(
                meta.at[mine], meta.at[1 + inner], m_send.at[0], m_recv.at[1 + inner],
                {"ep": partner},
            )
        return remote(meta.at[1], meta.at[3], m_send.at[1], m_recv.at[3], {"ep": far})

    def part_copy(kind, c):
        if kind == 2:
            return remote(
                fp_recv.at[1, c], fp_recv.at[1, c], q_send.at[2, c], q_recv.at[1, c], {"ep": mate}
            )
        return remote(
            fp_send.at[kind, c], fp_recv.at[kind, c], q_send.at[kind, c], q_recv.at[kind, c],
            {"ep": far},
        )

    def await_rows(g, c):
        await_bytes(held.at[g, c], n_recv.at[g, c])

    def await_meta(g):
        await_bytes(meta.at[g], m_recv.at[g])

    def await_part(kind, c):
        await_bytes(fp_recv.at[kind, c], q_recv.at[kind, c])

    def relay(c):
        await_rows(1, c)
        rows_copy(1, c).start()
        pick(1, 0, c)

    def accept(g, c):
        await_rows(g, c)
        pick(g, 1, c)
        pick(g, 0, c)

    def share(g, c):
        fp_send[g - 2, c] = (mix(g, 0, c) + mix(g, 1, c)).astype(jnp.bfloat16)
        part_copy(g - 2, c).start()

    meta_copy(0).start()
    for c in every:
        xs = x_ref[:, c * cw : (c + 1) * cw].astype(jnp.float32)
        held[mine, c] = (xs * scale * pre_ref[:, c * cw : (c + 1) * cw]).astype(jnp.bfloat16)
        if c == 0:
            rows_copy(0, c).start()
        else:
            on_outer(rows_copy(0, c).start)
    place(mine, (0, 1))

    @pl.loop(0, CHUNKS)
    def _(c):
        pick(mine, 0, c)
        on_inner(lambda: pick(0, 1, c))

    @on_inner
    def _():
        await_meta(1)
        meta_copy(1).start()
        place(1, (0,))

        @pl.loop(0, 2)
        def _(c):
            relay(c)

        await_meta(3)
        place(3, (0, 1))
        accept(3, 0)

    received_in_plane(mine)
    local_copies[0].wait()
    local_copies[1].wait()
    expand(mine, 0)

    @on_inner
    def _():
        await_meta(2)
        place(2, (0, 1))

        @pl.loop(2, CHUNKS)
        def _(c):
            relay(c)

            @pl.when(c == CHUNKS - 1)
            def _():
                for d in range(1, CHUNKS):
                    rows_copy(0, d).start()

            accept(3, c - 1)

    def await_peers(w):
        for copy in peer_copies[w]:
            copy.wait()

    on_outer(lambda: received_crossed(0))
    on_inner(lambda: await_peers(0))
    on_inner(lambda: await_peers(1))
    expand(0, inner)
    on_inner(lambda: received_in_plane(1))
    on_outer(lambda: await_peers(0))
    on_outer(lambda: await_peers(1))
    expand(inner, outer)

    @on_inner
    def _():
        accept(3, CHUNKS - 1)
        accept(2, 0)

    def await_down():
        local_copies[2].wait()
        await_peers(2)

    @on_outer
    def _():
        await_down()
        contract(0, 1)

    expand(1, 1)
    on_outer(lambda: contract(1, 0))
    received(3)
    expand(3, 0)
    on_inner(lambda: accept(2, 1))
    expand(3, 1)
    on_inner(await_down)
    contract(3, outer)

    @on_inner
    def _():
        @pl.loop(2, CHUNKS)
        def _(c):
            accept(2, c)

        @pl.loop(0, 2)
        def _(c):
            share(3, c)

        contract(1, 0)

    received(2)
    expand(2, 0)
    on_inner(lambda: share(3, 2))
    expand(2, 1)
    on_inner(lambda: share(3, 3))
    contract(2, outer)

    @on_inner
    def _():
        contract(0, 0)

        @pl.loop(0, CHUNKS)
        def _(c):
            value = mix(1, 0, c)
            await_part(1, c)
            fp_recv[1, c] = (value + fp_recv[1, c].astype(jnp.float32)).astype(jnp.bfloat16)
            part_copy(2, c).start()
            share(2, c)

    @pl.loop(0, CHUNKS)
    def _(c):
        mixed[c] = mix(mine, 0, c)

        @on_inner
        def _():
            mixed[c] = mixed[c] + mix(0, 1, c)

    squares = jnp.zeros((tokens, 1), jnp.float32)
    for c in every:
        await_part(mine, c)
        total = mixed[c] + fp_recv[mine, c].astype(jnp.float32)
        mixed[c] = total
        squares = squares + jnp.sum(total * total, axis=-1, keepdims=True)
    scale = lax.rsqrt(squares / width + EPSILON)
    for c in every:
        at = slice(c * cw, (c + 1) * cw)
        out_ref[:, at] = (mixed[c] * scale * post_ref[:, at]).astype(jnp.bfloat16)

    meta_copy(0).wait_send()
    on_inner(meta_copy(1).wait_send)

    @pl.loop(0, CHUNKS)
    def _(c):
        def in_plane(g):
            own = pl.ds(cap, rows - cap)
            await_bytes(send.at[2 * g, c, own], d_send.at[2 * g, c])
            await_bytes(recv.at[g, c, own], r_send.at[g, c])

        rows_copy(0, c).wait_send()
        in_plane(mine)

        @on_inner
        def _():
            rows_copy(1, c).wait_send()
            for kind in range(3):
                part_copy(kind, c).wait_send()
            for g in (1, 2, 3):
                in_plane(g)
            for g in (0, 2, 3):
                await_bytes(send.at[2 * g + 1, c], d_send.at[2 * g + 1, c])

        @on_outer
        def _():
            for g in (0, 2, 3):
                await_bytes(recv.at[g, c], r_send.at[g, c])


def local(inputs, pre_gain, expert_ids, route_weights, gate_proj, up_proj, down_proj, post_gain):
    tokens, width = inputs.shape
    choices = expert_ids.shape[1]
    n = lax.axis_size("ep")
    tps = lax.axis_size("tp")
    cap = 3 * tokens * choices // (2 * n * gate_proj.shape[0])
    cap = -(-cap // 16) * 16
    rows = n // PLANES * cap
    cw = width // CHUNKS
    fh = gate_proj.shape[2]
    bf16, f32 = jnp.bfloat16, jnp.float32
    vmem = pl.BlockSpec(memory_space=pltpu.VMEM)
    hbm = pl.BlockSpec(memory_space=pl.ANY)
    dma = pltpu.SemaphoreType.DMA
    return pl.pallas_call(
        functools.partial(kernel, n, tps, cap),
        out_shape=jax.ShapeDtypeStruct((tokens, width), bf16),
        in_specs=[hbm, vmem, vmem, vmem, hbm, hbm, hbm, vmem],
        out_specs=vmem,
        scratch_shapes=[
            pltpu.VMEM((tokens, width), bf16),
            pltpu.VMEM((tps, width, fh), bf16),
            pltpu.VMEM((tps, width, fh), bf16),
            pltpu.VMEM((tps, fh, width), bf16),
            pltpu.VMEM((4, CHUNKS, tokens, cw), bf16),
            pltpu.VMEM((4, 8, tokens), f32),
            pltpu.VMEM((8, CHUNKS, rows, cw), bf16),
            pltpu.VMEM((4, CHUNKS, rows, cw), bf16),
            pltpu.VMEM((8, CHUNKS, rows, cw), bf16),
            pltpu.VMEM((2, CHUNKS, tokens, cw), bf16),
            pltpu.VMEM((2, CHUNKS, tokens, cw), bf16),
            pltpu.VMEM((CHUNKS, tokens, cw), f32),
            pltpu.VMEM((4, tps, rows, fh), bf16),
            pltpu.VMEM((8, 8, tokens), f32),
            dma, dma((3,)), dma((3, tps - 1)), dma((3, tps - 1)),
            dma((2, CHUNKS)), dma((4, CHUNKS)), dma((2,)), dma((4,)),
            dma((8, CHUNKS)), dma((4, CHUNKS)), dma((4, CHUNKS)), dma((8, CHUNKS)),
            dma((3, CHUNKS)), dma((2, CHUNKS)),
        ],
        compiler_params=pltpu.CompilerParams(
            collective_id=0, has_side_effects=True, vmem_limit_bytes=67043328
        ),
    )(
        inputs, pre_gain[None, :], expert_ids.T, route_weights.T,
        gate_proj, up_proj, down_proj, post_gain[None, :],
    )


def solution(mesh):
    in_specs = (
        P(("ep", "tp"), None),
        P(),
        P(("ep", "tp"), None),
        P(("ep", "tp"), None),
        P("ep", None, "tp"),
        P("ep", None, "tp"),
        P("ep", "tp", None),
        P(),
    )
    out_specs = P(("ep", "tp"), None)
    return jax.shard_map(local, mesh=mesh, in_specs=in_specs, out_specs=out_specs, check_vma=False)
```

time: 143 us -> 120 us (0.84)
  the two profiles are of different devices: /device:TPU:0 before, /device:TPU:8 now
where the time goes in v1:
time: 120 us; the launch traced here: 119 us
  Pallas kernels  117 us (98%)
  local copies, waits for them, and re-layouts  2.3 us (2%)
    pallas_call x1, Pallas kernels, local(): pl.pallas_call(functools.partial(kernel, n, tps, cap), out_shape=jax.Shap...  117 us

profile of v1, /device:TPU:8, one launch (start us, length us, event | category | flops | bytes accessed | tf_op | source)
XLA Modules:
  0.0 118.9 jit_solution(12039609520385084933)
XLA Ops:
  0.0 116.6 %shard_map.82 = bf16[256,2048]{1,0:T(8,128)(2,1)} custom-call(bf16[256,2048]{1,0:T(8,128)(2,1)} %x_hbm.1, f32[1,2048]{1,0:T(1,128)} %bitcast.4, s32[2,256]{1,0:T(2,128)} %bitcast.6, f32[2,256]{1,0:T(2,128)} %bitcast.7, bf16[1,2048,1024]{2,1,0:T(8,128)(2,1)} %gate_ref.1, bf16[1,2048,1024]{2,1,0:T(8,128)(2,1)} %up_ref.1, bf16[1,1024,2048]{2,1,0:T(8,128)(2,1)} %down_ref.1, ...), custom_call_target="tpu_custom_call" | custom-call | tf_op jit(solution)/shard_map/pallas_call | solution.py:480
  116.6 2.3 %copy.10 = bf16[256,2048]{1,0:T(8,128)(2,1)} copy(bf16[256,2048]{1,0:T(8,128)(2,1)} %shard_map.82) | data formatting | bytes 2097152

commit v2 on v1

--- a/solution.py
+++ b/solution.py
@@ -11,6 +11,7 @@
 LIMIT = 7.0
 ALPHA = 1.702
 CHUNKS = 4
+DIRECT = 2
 TILE = 256
 PLANES = 4
 MESH = pl.DeviceIdType.MESH
@@ -28,11 +29,11 @@
 
 def kernel(
     n, tps, cap,
-    x_hbm, pre_ref, ids_ref, route_ref, gate_ref, up_ref, down_ref, post_ref, out_ref,
+    x_hbm, pre_ref, ids_ref, route_ref, gate_ref, up_ref, down_ref, post_ref, out_hbm,
     x_ref, gate_v, up_v, down_v, held, meta, send, recv, ret,
     fp_send, fp_recv, mixed, hidden, places,
     x_sem, w_local, w_send, w_recv, n_send, n_recv, m_send, m_recv,
-    d_send, d_recv, r_send, r_recv, q_send, q_recv,
+    d_send, d_recv, r_send, r_recv, f_send, q_send, q_recv, o_sem,
 ):
     tokens, width = x_ref.shape
     pz = n // PLANES
@@ -91,8 +92,6 @@
     def _():
         greet({"ep": far})
 
-    pl.semaphore_wait(barrier, 2 * pz - 1 + tps - 1 + inner)
-
     def remote(src, dst, ss, rs, where):
         return pltpu.make_async_remote_copy(
             src_ref=src, dst_ref=dst, send_sem=ss, recv_sem=rs,
@@ -112,10 +111,6 @@
         ]
         for w, (src, dst) in enumerate(weights)
     ]
-    for copies in peer_copies:
-        for copy in copies:
-            copy.start()
-
     meta[mine, 0:2, :] = ids_ref[...].astype(jnp.float32)
     meta[mine, 2:4, :] = route_ref[...]
     meta[mine, 4:8, :] = jnp.zeros((4, tokens), jnp.float32)
@@ -204,11 +199,10 @@
                 up += dot(recv[g, c], up_v[h, c * cw : (c + 1) * cw, at])
             hidden[g, h, :, at] = activate(gate, up)
 
-    def contract(g, t):
-        k = 2 * g + t
+    def contract(g, k, t, chunks=(0, CHUNKS)):
         base = own_base + t * (mate_base - own_base)
 
-        @pl.loop(0, CHUNKS)
+        @pl.loop(*chunks)
         def _(c):
             for s in range(cw // TILE):
                 lo = s * TILE
@@ -294,19 +288,35 @@
         pick(g, 1, c)
         pick(g, 0, c)
 
+    def forward_copy(g, c):
+        k = 2 * g + 1
+        return remote(
+            ret.at[k, c], ret.at[k, c], f_send.at[g - 2, c], r_recv.at[k, c], {"ep": mate}
+        )
+
+    def forward(g, chunks):
+        @pl.loop(*chunks)
+        def _(c):
+            k = 2 * g + 1
+            await_bytes(ret.at[k, c, pl.ds(cap, rows - cap)], r_recv.at[k, c])
+            forward_copy(g, c).start()
+
     def share(g, c):
         fp_send[g - 2, c] = (mix(g, 0, c) + mix(g, 1, c)).astype(jnp.bfloat16)
         part_copy(g - 2, c).start()
 
-    meta_copy(0).start()
     for c in every:
         xs = x_ref[:, c * cw : (c + 1) * cw].astype(jnp.float32)
         held[mine, c] = (xs * scale * pre_ref[:, c * cw : (c + 1) * cw]).astype(jnp.bfloat16)
-        if c == 0:
-            rows_copy(0, c).start()
-        else:
-            on_outer(rows_copy(0, c).start)
     place(mine, (0, 1))
+    pl.semaphore_wait(barrier, 2 * pz - 1 + tps - 1 + inner)
+    meta_copy(0).start()
+    rows_copy(0, 0).start()
+    for c in range(1, CHUNKS):
+        on_outer(rows_copy(0, c).start)
+    for copies in peer_copies:
+        for copy in copies:
+            copy.start()
 
     @pl.loop(0, CHUNKS)
     def _(c):
@@ -373,55 +383,56 @@
     @on_outer
     def _():
         await_down()
-        contract(0, 1)
+        contract(0, 1, 1)
 
     expand(1, 1)
-    on_outer(lambda: contract(1, 0))
+    on_outer(lambda: contract(1, 2, 0))
     received(3)
     expand(3, 0)
     on_inner(lambda: accept(2, 1))
     expand(3, 1)
     on_inner(await_down)
-    contract(3, outer)
+    contract(3, 6 + outer, outer, (0, DIRECT))
+    on_inner(lambda: accept(2, 2))
+
+    @on_outer
+    def _():
+        contract(3, 7, 0, (DIRECT, CHUNKS))
+        forward(3, (DIRECT, CHUNKS))
 
     @on_inner
     def _():
-        @pl.loop(2, CHUNKS)
-        def _(c):
-            accept(2, c)
-
-        @pl.loop(0, 2)
-        def _(c):
-            share(3, c)
-
-        contract(1, 0)
+        accept(2, 3)
+        share(3, 0)
+        contract(3, 6, 0, (DIRECT, CHUNKS))
+        share(3, 1)
+        contract(1, 3, 1)
 
     received(2)
     expand(2, 0)
     on_inner(lambda: share(3, 2))
     expand(2, 1)
     on_inner(lambda: share(3, 3))
-    contract(2, outer)
+    contract(2, 4 + outer, 0)
+    on_outer(lambda: forward(2, (0, CHUNKS)))
 
     @on_inner
     def _():
-        contract(0, 0)
+        contract(0, 0, 0)
 
         @pl.loop(0, CHUNKS)
         def _(c):
-            value = mix(1, 0, c)
             await_part(1, c)
-            fp_recv[1, c] = (value + fp_recv[1, c].astype(jnp.float32)).astype(jnp.bfloat16)
             part_copy(2, c).start()
             share(2, c)
 
     @pl.loop(0, CHUNKS)
     def _(c):
-        mixed[c] = mix(mine, 0, c)
-
-        @on_inner
-        def _():
-            mixed[c] = mixed[c] + mix(0, 1, c)
+        mixed[c] = mix(mine, 0, c) + mix(mine, 1, c)
+
+    def out_copy(c):
+        at = pl.ds(c * cw, cw)
+        return pltpu.make_async_copy(x_ref.at[:, at], out_hbm.at[:, at], o_sem.at[c])
 
     squares = jnp.zeros((tokens, 1), jnp.float32)
     for c in every:
@@ -432,7 +443,8 @@
     scale = lax.rsqrt(squares / width + EPSILON)
     for c in every:
         at = slice(c * cw, (c + 1) * cw)
-        out_ref[:, at] = (mixed[c] * scale * post_ref[:, at]).astype(jnp.bfloat16)
+        x_ref[:, at] = (mixed[c] * scale * post_ref[:, at]).astype(jnp.bfloat16)
+        out_copy(c).start()
 
     meta_copy(0).wait_send()
     on_inner(meta_copy(1).wait_send)
@@ -441,10 +453,14 @@
     def _(c):
         def in_plane(g):
             own = pl.ds(cap, rows - cap)
+            await_bytes(recv.at[g, c, own], r_send.at[g, c])
+
+        def picked(g):
+            own = pl.ds(cap, rows - cap)
             await_bytes(send.at[2 * g, c, own], d_send.at[2 * g, c])
-            await_bytes(recv.at[g, c, own], r_send.at[g, c])
 
         rows_copy(0, c).wait_send()
+        picked(mine)
         in_plane(mine)
 
         @on_inner
@@ -453,14 +469,30 @@
             for kind in range(3):
                 part_copy(kind, c).wait_send()
             for g in (1, 2, 3):
+                picked(g)
+            for g in (2, 3):
                 in_plane(g)
+            await_bytes(recv.at[1, c], r_send.at[1, c])
             for g in (0, 2, 3):
                 await_bytes(send.at[2 * g + 1, c], d_send.at[2 * g + 1, c])
 
         @on_outer
         def _():
-            for g in (0, 2, 3):
-                await_bytes(recv.at[g, c], r_send.at[g, c])
+            await_bytes(recv.at[0, c], r_send.at[0, c])
+            in_plane(2)
+            forward_copy(2, c).wait_send()
+
+            @pl.when(c < DIRECT)
+            def _():
+                await_bytes(recv.at[3, c], r_send.at[3, c])
+
+            @pl.when(c >= DIRECT)
+            def _():
+                in_plane(3)
+                forward_copy(3, c).wait_send()
+
+    for c in every:
+        out_copy(c).wait()
 
 
 def local(inputs, pre_gain, expert_ids, route_weights, gate_proj, up_proj, down_proj, post_gain):
@@ -481,7 +513,7 @@
         functools.partial(kernel, n, tps, cap),
         out_shape=jax.ShapeDtypeStruct((tokens, width), bf16),
         in_specs=[hbm, vmem, vmem, vmem, hbm, hbm, hbm, vmem],
-        out_specs=vmem,
+        out_specs=hbm,
         scratch_shapes=[
             pltpu.VMEM((tokens, width), bf16),
             pltpu.VMEM((tps, width, fh), bf16),
@@ -500,7 +532,7 @@
             dma, dma((3,)), dma((3, tps - 1)), dma((3, tps - 1)),
             dma((2, CHUNKS)), dma((4, CHUNKS)), dma((2,)), dma((4,)),
             dma((8, CHUNKS)), dma((4, CHUNKS)), dma((4, CHUNKS)), dma((8, CHUNKS)),
-            dma((3, CHUNKS)), dma((2, CHUNKS)),
+            dma((2, CHUNKS)), dma((3, CHUNKS)), dma((2, CHUNKS)), dma((CHUNKS,)),
         ],
         compiler_params=pltpu.CompilerParams(
             collective_id=0, has_side_effects=True, vmem_limit_bytes=67043328

time: 120 us -> 107 us (0.89)
  Pallas kernels: 117 us -> 104 us
    pallas_call x1, Pallas kernels: 117 us -> 104 us  [local(): pl.pallas_call(functools.partial(kernel, n, tps, cap), out_shape=jax.Shap...]
where the time goes in v2:
time: 107 us; the launch traced here: 106 us
  Pallas kernels  104 us (97%)
  local copies, waits for them, and re-layouts  2.3 us (2%)
    pallas_call x1, Pallas kernels, local(): pl.pallas_call(functools.partial(kernel, n, tps, cap), out_shape=jax.Shap...  104 us
    unnamed x1, local copies, waits for them, and re-layouts  2.3 us

profile of v2, /device:TPU:8, one launch (start us, length us, event | category | flops | bytes accessed | tf_op | source)
XLA Modules:
  0.0 106.0 jit_solution(13046579864300655675)
XLA Ops:
  0.0 103.7 %shard_map.82 = bf16[256,2048]{1,0:T(8,128)(2,1)} custom-call(bf16[256,2048]{1,0:T(8,128)(2,1)} %x_hbm.1, f32[1,2048]{1,0:T(1,128)} %bitcast.4, s32[2,256]{1,0:T(2,128)} %bitcast.6, f32[2,256]{1,0:T(2,128)} %bitcast.7, bf16[1,2048,1024]{2,1,0:T(8,128)(2,1)} %gate_ref.1, bf16[1,2048,1024]{2,1,0:T(8,128)(2,1)} %up_ref.1, bf16[1,1024,2048]{2,1,0:T(8,128)(2,1)} %down_ref.1, ...), custom_call_target="tpu_custom_call" | custom-call | tf_op jit(solution)/shard_map/pallas_call | solution.py:512
  103.7 2.3 %copy.10 = bf16[256,2048]{1,0:T(8,128)(2,1)} copy(bf16[256,2048]{1,0:T(8,128)(2,1)} %shard_map.82) | data formatting | bytes 2097152

commit v3 on v2

--- a/solution.py
+++ b/solution.py
@@ -10,8 +10,12 @@
 EPSILON = 1e-06
 LIMIT = 7.0
 ALPHA = 1.702
-CHUNKS = 4
-DIRECT = 2
+CHUNKS = 8
+DIRECT = 4
+EARLY = 2
+LATER = 6
+BLOCKS = 4
+PAIR = 2
 TILE = 256
 PLANES = 4
 MESH = pl.DeviceIdType.MESH
@@ -31,9 +35,9 @@
     n, tps, cap,
     x_hbm, pre_ref, ids_ref, route_ref, gate_ref, up_ref, down_ref, post_ref, out_hbm,
     x_ref, gate_v, up_v, down_v, held, meta, send, recv, ret,
-    fp_send, fp_recv, mixed, hidden, places,
+    fp_send, fp_recv, mixed, hidden, places, mixers,
     x_sem, w_local, w_send, w_recv, n_send, n_recv, m_send, m_recv,
-    d_send, d_recv, r_send, r_recv, f_send, q_send, q_recv, o_sem,
+    d_send, d_recv, r_send, r_near, r_recv, f_send, q_send, q_recv, o_sem,
 ):
     tokens, width = x_ref.shape
     pz = n // PLANES
@@ -143,14 +147,15 @@
             + (places[k, 1:2, :] == at).astype(jnp.float32)
         ).astype(jnp.bfloat16)
 
-    def mixer(k):
+    def prepare(k):
         columns = places[k].T
         at = lax.broadcasted_iota(jnp.int32, (1, rows), 1).astype(jnp.float32)
         w = jnp.where(columns[:, 0:1] == at, columns[:, 2:3], 0.0) + jnp.where(
             columns[:, 1:2] == at, columns[:, 3:4], 0.0
         )
         high = w.astype(jnp.bfloat16)
-        return high, (w - high.astype(jnp.float32)).astype(jnp.bfloat16)
+        mixers[k, 0] = high
+        mixers[k, 1] = (w - high.astype(jnp.float32)).astype(jnp.bfloat16)
 
     def block_of(j):
         return pl.ds(pl.multiple_of(j * cap, cap), cap)
@@ -169,27 +174,23 @@
         def _(j):
             remote(
                 send.at[k, c, block_of(j)], recv.at[g, c, block_of(j)],
-                d_send.at[k, c], d_recv.at[g, c], {"ep": ring(base, j)},
+                d_send.at[k], d_recv.at[g], {"ep": ring(base, j)},
             ).start()
 
     def received_in_plane(g):
-        @pl.loop(0, CHUNKS)
-        def _(c):
-            await_bytes(recv.at[g, c, pl.ds(cap, rows - cap)], d_recv.at[g, c])
+        await_bytes(recv.at[g, :, pl.ds(cap, rows - cap)], d_recv.at[g])
 
     def received_crossed(g):
-        @pl.loop(0, CHUNKS)
-        def _(c):
-            await_bytes(recv.at[g, c], d_recv.at[g, c])
+        await_bytes(recv.at[g], d_recv.at[g])
 
     def received(g):
         on_inner(lambda: received_in_plane(g))
         on_outer(lambda: received_crossed(g))
 
-    def expand(g, i):
+    def expand(g, i, first=0, tiles=fh // TILE):
         h = lax.rem(core + i, tps)
 
-        @pl.loop(0, fh // TILE)
+        @pl.loop(first, first + tiles)
         def _(t):
             at = pl.ds(pl.multiple_of(t * TILE, TILE), TILE)
             gate = jnp.zeros((rows, TILE), jnp.float32)
@@ -199,39 +200,45 @@
                 up += dot(recv[g, c], up_v[h, c * cw : (c + 1) * cw, at])
             hidden[g, h, :, at] = activate(gate, up)
 
+    def came(g, k, c):
+        return r_near.at[k] if isinstance(g, int) and g < 2 else r_recv.at[k - 4, c]
+
     def contract(g, k, t, chunks=(0, CHUNKS)):
         base = own_base + t * (mate_base - own_base)
 
-        @pl.loop(*chunks)
-        def _(c):
-            for s in range(cw // TILE):
-                lo = s * TILE
-                total = jnp.zeros((rows, TILE), jnp.float32)
-                for h in range(tps):
-                    at = pl.ds(pl.multiple_of(c * cw + lo, TILE), TILE)
-                    part = dot(hidden[g, h], down_v[h, :, at])
-                    total += part.astype(jnp.bfloat16).astype(jnp.float32)
-                recv[g, c, :, lo : lo + TILE] = total.astype(jnp.bfloat16)
+        @pl.loop(chunks[0] // PAIR, chunks[1] // PAIR)
+        def _(p):
+            total = jnp.zeros((rows, PAIR * cw), jnp.float32)
+            for h in range(tps):
+                at = pl.ds(pl.multiple_of(p * PAIR * cw, PAIR * cw), PAIR * cw)
+                part = dot(hidden[g, h], down_v[h, :, at])
+                total += part.astype(jnp.bfloat16).astype(jnp.float32)
+            total = total.astype(jnp.bfloat16)
+            for q in range(PAIR):
+                recv[g, PAIR * p + q] = total[:, q * cw : (q + 1) * cw]
 
             @pl.when(t == 0)
             def _():
-                ret[k, c, 0:cap, :] = recv[g, c, 0:cap, :]
-
-            @pl.loop(1 - t, pz)
-            def _(j):
-                remote(
-                    recv.at[g, c, block_of(j)], ret.at[k, c, block_of(j)],
-                    r_send.at[g, c], r_recv.at[k, c], {"ep": ring(base, pz - j)},
-                ).start()
-
-    def mix(g, t, c):
+                for q in range(PAIR):
+                    ret[k, PAIR * p + q, 0:cap, :] = total[0:cap, q * cw : (q + 1) * cw]
+
+            for q in range(PAIR):
+                c = PAIR * p + q
+
+                @pl.loop(1 - t, pz)
+                def _(j):
+                    remote(
+                        recv.at[g, c, block_of(j)], ret.at[k, c, block_of(j)],
+                        r_send.at[g], came(g, k, c), {"ep": ring(base, pz - j)},
+                    ).start()
+
+    def mix(k, c):
+        return dot(mixers[k, 0], ret[k, c]) + dot(mixers[k, 1], ret[k, c])
+
+    def await_far(g, t, c):
         k = 2 * g + t
-        high, low = mixer(k)
-        if t == 0:
-            await_bytes(ret.at[k, c, pl.ds(cap, rows - cap)], r_recv.at[k, c])
-        else:
-            await_bytes(ret.at[k, c], r_recv.at[k, c])
-        return dot(high, ret[k, c]) + dot(low, ret[k, c])
+        part = ret.at[k, c] if t else ret.at[k, c, pl.ds(cap, rows - cap)]
+        await_bytes(part, came(g, k, c))
 
     x_copy.wait()
     squares = jnp.zeros((tokens, 1), jnp.float32)
@@ -244,11 +251,11 @@
     def rows_copy(step, c):
         if step == 0:
             return remote(
-                held.at[mine, c], held.at[1 + inner, c], n_send.at[0, c], n_recv.at[1 + inner, c],
+                held.at[mine, c], held.at[1 + inner, c], n_send.at[0], n_recv.at[inner, c],
                 {"ep": partner},
             )
         return remote(
-            held.at[1, c], held.at[3, c], n_send.at[1, c], n_recv.at[3, c], {"ep": far}
+            held.at[1, c], held.at[3, c], n_send.at[1], n_recv.at[2, c], {"ep": far}
         )
 
     def meta_copy(step):
@@ -262,15 +269,15 @@
     def part_copy(kind, c):
         if kind == 2:
             return remote(
-                fp_recv.at[1, c], fp_recv.at[1, c], q_send.at[2, c], q_recv.at[1, c], {"ep": mate}
+                fp_recv.at[1, c], fp_recv.at[1, c], q_send.at[2], q_recv.at[1, c], {"ep": mate}
             )
         return remote(
-            fp_send.at[kind, c], fp_recv.at[kind, c], q_send.at[kind, c], q_recv.at[kind, c],
+            fp_send.at[kind, c], fp_recv.at[kind, c], q_send.at[kind], q_recv.at[kind, c],
             {"ep": far},
         )
 
     def await_rows(g, c):
-        await_bytes(held.at[g, c], n_recv.at[g, c])
+        await_bytes(held.at[g, c], n_recv.at[g - 1, c])
 
     def await_meta(g):
         await_bytes(meta.at[g], m_recv.at[g])
@@ -291,18 +298,20 @@
     def forward_copy(g, c):
         k = 2 * g + 1
         return remote(
-            ret.at[k, c], ret.at[k, c], f_send.at[g - 2, c], r_recv.at[k, c], {"ep": mate}
+            ret.at[k, c], ret.at[k, c], f_send.at[g - 2], came(g, k, c), {"ep": mate}
         )
 
     def forward(g, chunks):
         @pl.loop(*chunks)
         def _(c):
             k = 2 * g + 1
-            await_bytes(ret.at[k, c, pl.ds(cap, rows - cap)], r_recv.at[k, c])
+            await_bytes(ret.at[k, c, pl.ds(cap, rows - cap)], came(g, k, c))
             forward_copy(g, c).start()
 
     def share(g, c):
-        fp_send[g - 2, c] = (mix(g, 0, c) + mix(g, 1, c)).astype(jnp.bfloat16)
+        await_far(g, 0, c)
+        await_far(g, 1, c)
+        fp_send[g - 2, c] = (mix(2 * g, c) + mix(2 * g + 1, c)).astype(jnp.bfloat16)
         part_copy(g - 2, c).start()
 
     for c in every:
@@ -310,10 +319,16 @@
         held[mine, c] = (xs * scale * pre_ref[:, c * cw : (c + 1) * cw]).astype(jnp.bfloat16)
     place(mine, (0, 1))
     pl.semaphore_wait(barrier, 2 * pz - 1 + tps - 1 + inner)
+    def await_peers(w):
+        for copy in peer_copies[w]:
+            copy.wait()
+
     meta_copy(0).start()
-    rows_copy(0, 0).start()
-    for c in range(1, CHUNKS):
-        on_outer(rows_copy(0, c).start)
+
+    @pl.loop(0, outer * CHUNKS + inner * EARLY)
+    def _(c):
+        rows_copy(0, c).start()
+
     for copies in peer_copies:
         for copy in copies:
             copy.start()
@@ -329,110 +344,191 @@
         meta_copy(1).start()
         place(1, (0,))
 
-        @pl.loop(0, 2)
+        @pl.loop(0, 3)
         def _(c):
             relay(c)
 
         await_meta(3)
         place(3, (0, 1))
         accept(3, 0)
-
-    received_in_plane(mine)
-    local_copies[0].wait()
-    local_copies[1].wait()
-    expand(mine, 0)
-
-    @on_inner
-    def _():
+        relay(3)
+        accept(3, 1)
+        received_in_plane(0)
+        local_copies[0].wait()
+        local_copies[1].wait()
         await_meta(2)
         place(2, (0, 1))
-
-        @pl.loop(2, CHUNKS)
+        some = tps * (fh // TILE) // (CHUNKS - 4)
+
+        @pl.loop(4, CHUNKS)
         def _(c):
             relay(c)
 
             @pl.when(c == CHUNKS - 1)
             def _():
-                for d in range(1, CHUNKS):
+                @pl.loop(EARLY, CHUNKS)
+                def _(d):
                     rows_copy(0, d).start()
 
-            accept(3, c - 1)
-
-    def await_peers(w):
-        for copy in peer_copies[w]:
-            copy.wait()
-
-    on_outer(lambda: received_crossed(0))
-    on_inner(lambda: await_peers(0))
-    on_inner(lambda: await_peers(1))
-    expand(0, inner)
-    on_inner(lambda: received_in_plane(1))
-    on_outer(lambda: await_peers(0))
-    on_outer(lambda: await_peers(1))
-    expand(inner, outer)
-
-    @on_inner
-    def _():
-        accept(3, CHUNKS - 1)
-        accept(2, 0)
+            accept(3, c - 2)
+
+            @pl.when(c == CHUNKS - 2)
+            def _():
+                await_peers(0)
+                await_peers(1)
+
+            tile = (c - 4) * some
+            expand(0, tile // (fh // TILE), lax.rem(tile, fh // TILE), some)
+
+    def accept_all(g, chunks):
+        @pl.loop(*chunks)
+        def _(c):
+            accept(g, c)
+
+    def share_all(g, chunks):
+        @pl.loop(*chunks)
+        def _(c):
+            share(g, c)
+
+    def pass_on(c):
+        await_part(1, c)
+        part_copy(2, c).start()
 
     def await_down():
         local_copies[2].wait()
         await_peers(2)
 
+    @on_inner
+    def _():
+        accept_all(3, (CHUNKS - 2, CHUNKS))
+        accept_all(2, (0, EARLY))
+        received_in_plane(1)
+        expand(1, 0)
+
     @on_outer
     def _():
+        received_crossed(0)
+        local_copies[0].wait()
+        local_copies[1].wait()
+        expand(0, 0)
+        await_peers(0)
+        await_peers(1)
+        for i in range(1, tps):
+            expand(0, i)
         await_down()
         contract(0, 1, 1)
-
-    expand(1, 1)
-    on_outer(lambda: contract(1, 2, 0))
+        received_in_plane(1)
+        for i in range(tps):
+            expand(1, i)
+
     received(3)
     expand(3, 0)
-    on_inner(lambda: accept(2, 1))
+    on_inner(lambda: accept_all(2, (2, 4)))
     expand(3, 1)
     on_inner(await_down)
     contract(3, 6 + outer, outer, (0, DIRECT))
-    on_inner(lambda: accept(2, 2))
 
     @on_outer
     def _():
         contract(3, 7, 0, (DIRECT, CHUNKS))
-        forward(3, (DIRECT, CHUNKS))
+        forward(3, (DIRECT, LATER))
 
     @on_inner
     def _():
-        accept(2, 3)
+        accept_all(2, (4, 6))
+        prepare(6)
+        prepare(7)
+        accept(2, 6)
         share(3, 0)
+        accept(2, 7)
+        share(3, 1)
+        expand(1, 1)
+        contract(1, 3, 1, (0, 4))
+        share(3, 2)
         contract(3, 6, 0, (DIRECT, CHUNKS))
-        share(3, 1)
-        contract(1, 3, 1)
+        share(3, 3)
+        contract(1, 3, 1, (4, CHUNKS))
+        prepare(4)
+        prepare(5)
 
     received(2)
     expand(2, 0)
-    on_inner(lambda: share(3, 2))
+    on_inner(lambda: share_all(3, (4, 6)))
+    on_outer(lambda: forward(3, (LATER, CHUNKS)))
     expand(2, 1)
-    on_inner(lambda: share(3, 3))
+    on_inner(lambda: share_all(3, (6, CHUNKS)))
     contract(2, 4 + outer, 0)
-    on_outer(lambda: forward(2, (0, CHUNKS)))
+
+    @on_outer
+    def _():
+        forward(2, (0, CHUNKS))
+        contract(1, 2, 0)
+
 
     @on_inner
     def _():
+        @pl.loop(0, 4)
+        def _(c):
+            pass_on(c)
+
+        share_all(2, (0, 2))
         contract(0, 0, 0)
 
-        @pl.loop(0, CHUNKS)
+        @pl.loop(2, CHUNKS)
         def _(c):
-            await_part(1, c)
-            part_copy(2, c).start()
             share(2, c)
+            pl.when(c < CHUNKS - 2)(lambda: pass_on(c + 2))
+
+    prepare(2 * mine)
+    prepare(2 * mine + 1)
+    await_bytes(ret.at[2 * mine, :, pl.ds(cap, rows - cap)], r_near.at[2 * mine])
+    await_bytes(ret.at[2 * mine + 1], r_near.at[2 * mine + 1])
 
     @pl.loop(0, CHUNKS)
     def _(c):
-        mixed[c] = mix(mine, 0, c) + mix(mine, 1, c)
-
-    def out_copy(c):
-        at = pl.ds(c * cw, cw)
-        return pltpu.make_async_copy(x_ref.at[:, at], out_hbm.at[:, at], o_sem.at[c])
+        mixed[c] = mix(2 * mine, c) + mix(2 * mine + 1, c)
+
+    meta_copy(0).wait_send()
+    on_inner(meta_copy(1).wait_send)
+    others = pl.ds(cap, rows - cap)
+
+    def picked(g):
+        await_bytes(send.at[2 * g, :, others], d_send.at[2 * g])
+
+    def in_plane(g):
+        await_bytes(recv.at[g, :, others], r_send.at[g])
+
+    picked(mine)
+    in_plane(mine)
+
+    @on_inner
+    def _():
+        await_bytes(held.at[0], n_send.at[0])
+        await_bytes(held.at[1], n_send.at[1])
+        for g in (1, 2, 3):
+            picked(g)
+        for g in (2, 3):
+            in_plane(g)
+        await_bytes(recv.at[1], r_send.at[1])
+        for g in (0, 2, 3):
+            await_bytes(send.at[2 * g + 1], d_send.at[2 * g + 1])
+        for kind in range(2):
+            await_bytes(fp_send.at[kind], q_send.at[kind])
+
+    @on_outer
+    def _():
+        await_bytes(held.at[1], n_send.at[0])
+        await_bytes(recv.at[0], r_send.at[0])
+        in_plane(2)
+        await_bytes(ret.at[5], f_send.at[0])
+        some = pl.ds(DIRECT, CHUNKS - DIRECT)
+        await_bytes(recv.at[3, pl.ds(0, DIRECT)], r_send.at[3])
+        await_bytes(recv.at[3, some, others], r_send.at[3])
+        await_bytes(ret.at[7, some], f_send.at[1])
+
+    def out_copy(b):
+        at = pl.ds(b * (tokens // BLOCKS), tokens // BLOCKS)
+        return pltpu.make_async_copy(x_ref.at[at], out_hbm.at[at], o_sem.at[b])
 
     squares = jnp.zeros((tokens, 1), jnp.float32)
     for c in every:
@@ -441,58 +537,17 @@
         mixed[c] = total
         squares = squares + jnp.sum(total * total, axis=-1, keepdims=True)
     scale = lax.rsqrt(squares / width + EPSILON)
-    for c in every:
-        at = slice(c * cw, (c + 1) * cw)
-        x_ref[:, at] = (mixed[c] * scale * post_ref[:, at]).astype(jnp.bfloat16)
-        out_copy(c).start()
-
-    meta_copy(0).wait_send()
-    on_inner(meta_copy(1).wait_send)
-
-    @pl.loop(0, CHUNKS)
-    def _(c):
-        def in_plane(g):
-            own = pl.ds(cap, rows - cap)
-            await_bytes(recv.at[g, c, own], r_send.at[g, c])
-
-        def picked(g):
-            own = pl.ds(cap, rows - cap)
-            await_bytes(send.at[2 * g, c, own], d_send.at[2 * g, c])
-
-        rows_copy(0, c).wait_send()
-        picked(mine)
-        in_plane(mine)
-
-        @on_inner
-        def _():
-            rows_copy(1, c).wait_send()
-            for kind in range(3):
-                part_copy(kind, c).wait_send()
-            for g in (1, 2, 3):
-                picked(g)
-            for g in (2, 3):
-                in_plane(g)
-            await_bytes(recv.at[1, c], r_send.at[1, c])
-            for g in (0, 2, 3):
-                await_bytes(send.at[2 * g + 1, c], d_send.at[2 * g + 1, c])
-
-        @on_outer
-        def _():
-            await_bytes(recv.at[0, c], r_send.at[0, c])
-            in_plane(2)
-            forward_copy(2, c).wait_send()
-
-            @pl.when(c < DIRECT)
-            def _():
-                await_bytes(recv.at[3, c], r_send.at[3, c])
-
-            @pl.when(c >= DIRECT)
-            def _():
-                in_plane(3)
-                forward_copy(3, c).wait_send()
-
-    for c in every:
-        out_copy(c).wait()
+    for b in range(BLOCKS):
+        own = slice(b * (tokens // BLOCKS), (b + 1) * (tokens // BLOCKS))
+        for c in every:
+            at = slice(c * cw, (c + 1) * cw)
+            x_ref[own, at] = (mixed[c, own] * scale[own] * post_ref[:, at]).astype(jnp.bfloat16)
+        out_copy(b).start()
+
+    on_inner(lambda: await_bytes(fp_recv.at[1], q_send.at[2]))
+
+    for b in range(BLOCKS):
+        out_copy(b).wait()
 
 
 def local(inputs, pre_gain, expert_ids, route_weights, gate_proj, up_proj, down_proj, post_gain):
@@ -529,10 +584,11 @@
             pltpu.VMEM((CHUNKS, tokens, cw), f32),
             pltpu.VMEM((4, tps, rows, fh), bf16),
             pltpu.VMEM((8, 8, tokens), f32),
+            pltpu.VMEM((8, 2, tokens, rows), bf16),
             dma, dma((3,)), dma((3, tps - 1)), dma((3, tps - 1)),
-            dma((2, CHUNKS)), dma((4, CHUNKS)), dma((2,)), dma((4,)),
-            dma((8, CHUNKS)), dma((4, CHUNKS)), dma((4, CHUNKS)), dma((8, CHUNKS)),
-            dma((2, CHUNKS)), dma((3, CHUNKS)), dma((2, CHUNKS)), dma((CHUNKS,)),
+            dma((2,)), dma((3, CHUNKS)), dma((2,)), dma((4,)),
+            dma((8,)), dma((4,)), dma((4,)), dma((4,)), dma((4, CHUNKS)),
+            dma((2,)), dma((3,)), dma((2, CHUNKS)), dma((BLOCKS,)),
         ],
         compiler_params=pltpu.CompilerParams(
             collective_id=0, has_side_effects=True, vmem_limit_bytes=67043328

time: 107 us -> 104 us (0.972); the launches traced: 106 us -> 104 us
  Pallas kernels: 104 us -> 102 us
    pallas_call x1, Pallas kernels: 104 us -> 102 us  [local(): pl.pallas_call(functools.partial(kernel, n, tps, cap), out_shape=jax.Shap...]
where the time goes in v3:
time: 104 us
  Pallas kernels  102 us (98%)
  local copies, waits for them, and re-layouts  2.3 us (2%)
    pallas_call x1, Pallas kernels, local(): pl.pallas_call(functools.partial(kernel, n, tps, cap), out_shape=jax.Shap...  102 us
    unnamed x1, local copies, waits for them, and re-layouts  2.3 us

profile of v3, /device:TPU:8, one launch (start us, length us, event | category | flops | bytes accessed | tf_op | source)
XLA Modules:
  0.0 104.1 jit_solution(13939180286747493725)
XLA Ops:
  0.0 101.8 %shard_map.82 = bf16[256,2048]{1,0:T(8,128)(2,1)} custom-call(bf16[256,2048]{1,0:T(8,128)(2,1)} %x_hbm.1, f32[1,2048]{1,0:T(1,128)} %bitcast.4, s32[2,256]{1,0:T(2,128)} %bitcast.6, f32[2,256]{1,0:T(2,128)} %bitcast.7, bf16[1,2048,1024]{2,1,0:T(8,128)(2,1)} %gate_ref.1, bf16[1,2048,1024]{2,1,0:T(8,128)(2,1)} %up_ref.1, bf16[1,1024,2048]{2,1,0:T(8,128)(2,1)} %down_ref.1, ...), custom_call_target="tpu_custom_call" | custom-call | tf_op jit(solution)/shard_map/pallas_call | solution.py:567
  101.8 2.3 %copy.10 = bf16[256,2048]{1,0:T(8,128)(2,1)} copy(bf16[256,2048]{1,0:T(8,128)(2,1)} %shard_map.82) | data formatting | bytes 2097152

commit v4 on v3

--- a/solution.py
+++ b/solution.py
@@ -13,6 +13,7 @@
 CHUNKS = 8
 DIRECT = 4
 EARLY = 2
+SPLIT = 6
 LATER = 6
 BLOCKS = 4
 PAIR = 2
@@ -33,13 +34,13 @@
 
 def kernel(
     n, tps, cap,
-    x_hbm, pre_ref, ids_ref, route_ref, gate_ref, up_ref, down_ref, post_ref, out_hbm,
-    x_ref, gate_v, up_v, down_v, held, meta, send, recv, ret,
-    fp_send, fp_recv, mixed, hidden, places, mixers,
+    x_hbm, pre_ref, ids_ref, route_ref, gate_ref, up_ref, down_ref, post_ref, out_ref,
+    gate_v, up_v, down_v, held, meta, send, recv, ret,
+    fp_send, fp_recv, acc, hidden, places, mixers,
     x_sem, w_local, w_send, w_recv, n_send, n_recv, m_send, m_recv,
-    d_send, d_recv, r_send, r_near, r_recv, f_send, q_send, q_recv, o_sem,
+    d_send, d_recv, r_send, r_near, r_recv, f_send, q_send, q_recv,
 ):
-    tokens, width = x_ref.shape
+    tokens, width = out_ref.shape
     pz = n // PLANES
     cw = width // CHUNKS
     rows = pz * cap
@@ -69,7 +70,7 @@
     def greet(device):
         pl.semaphore_signal(barrier, inc=1, device_id=device, device_id_type=MESH)
 
-    x_copy = pltpu.make_async_copy(x_hbm, x_ref, x_sem)
+    x_copy = pltpu.make_async_copy(x_hbm, out_ref, x_sem)
     x_copy.start()
     weights = ((gate_ref, gate_v), (up_ref, up_v), (down_ref, down_v))
     local_copies = [
@@ -147,34 +148,38 @@
             + (places[k, 1:2, :] == at).astype(jnp.float32)
         ).astype(jnp.bfloat16)
 
-    def prepare(k):
+    def prepare(k, r):
         columns = places[k].T
         at = lax.broadcasted_iota(jnp.int32, (1, rows), 1).astype(jnp.float32)
         w = jnp.where(columns[:, 0:1] == at, columns[:, 2:3], 0.0) + jnp.where(
             columns[:, 1:2] == at, columns[:, 3:4], 0.0
         )
         high = w.astype(jnp.bfloat16)
-        mixers[k, 0] = high
-        mixers[k, 1] = (w - high.astype(jnp.float32)).astype(jnp.bfloat16)
+        mixers[r, 0] = high
+        mixers[r, 1] = (w - high.astype(jnp.float32)).astype(jnp.bfloat16)
 
     def block_of(j):
         return pl.ds(pl.multiple_of(j * cap, cap), cap)
 
+    def sent(g, t):
+        return 2 * g + t - (1 if isinstance(g, int) and g > 1 else 0)
+
     def pick(g, t, c):
-        k = 2 * g + t
-        picked = dot(picker(k), held[g, c]).astype(jnp.bfloat16)
+        k = sent(g, t)
+        picked = dot(picker(2 * g + t), held[g, c]).astype(jnp.bfloat16)
         if t == 0:
             recv[g, c, 0:cap, :] = picked[0:cap]
             send[k, c, cap:rows, :] = picked[cap:rows]
         else:
             send[k, c] = picked
         base = mate_base if t else own_base
+        late = c // SPLIT if isinstance(g, int) and g == 3 else 0
 
         @pl.loop(1 - t, pz)
         def _(j):
             remote(
                 send.at[k, c, block_of(j)], recv.at[g, c, block_of(j)],
-                d_send.at[k], d_recv.at[g], {"ep": ring(base, j)},
+                d_send.at[k], d_recv.at[g + late], {"ep": ring(base, j)},
             ).start()
 
     def received_in_plane(g):
@@ -186,6 +191,40 @@
     def received(g):
         on_inner(lambda: received_in_plane(g))
         on_outer(lambda: received_crossed(g))
+
+    def received_part(late):
+        part = pl.ds(SPLIT * late, SPLIT + late * (CHUNKS - 2 * SPLIT))
+        on_inner(lambda: await_bytes(recv.at[3, part, pl.ds(cap, rows - cap)], d_recv.at[3 + late]))
+        on_outer(lambda: await_bytes(recv.at[3, part], d_recv.at[3 + late]))
+
+    def begin(i):
+        h = lax.rem(core + i, tps)
+
+        @pl.loop(0, fh // TILE)
+        def _(t):
+            at = pl.ds(pl.multiple_of(t * TILE, TILE), TILE)
+            gate = jnp.zeros((rows, TILE), jnp.float32)
+            up = jnp.zeros((rows, TILE), jnp.float32)
+            for c in range(SPLIT):
+                gate += dot(recv[3, c], gate_v[h, c * cw : (c + 1) * cw, at])
+                up += dot(recv[3, c], up_v[h, c * cw : (c + 1) * cw, at])
+            acc[2 * i, 0:rows, at] = gate
+            acc[2 * i + 1, 0:rows, at] = up
+
+    def complete(i):
+        h = lax.rem(core + i, tps)
+
+        @pl.loop(0, fh // TILE)
+        def _(t):
+            at = pl.ds(pl.multiple_of(t * TILE, TILE), TILE)
+            gate = jnp.zeros((rows, TILE), jnp.float32)
+            up = jnp.zeros((rows, TILE), jnp.float32)
+            for c in range(SPLIT, CHUNKS):
+                gate += dot(recv[3, c], gate_v[h, c * cw : (c + 1) * cw, at])
+                up += dot(recv[3, c], up_v[h, c * cw : (c + 1) * cw, at])
+            gate += acc[2 * i, 0:rows, at]
+            up += acc[2 * i + 1, 0:rows, at]
+            hidden[3, h, :, at] = activate(gate, up)
 
     def expand(g, i, first=0, tiles=fh // TILE):
         h = lax.rem(core + i, tps)
@@ -201,7 +240,7 @@
             hidden[g, h, :, at] = activate(gate, up)
 
     def came(g, k, c):
-        return r_near.at[k] if isinstance(g, int) and g < 2 else r_recv.at[k - 4, c]
+        return r_near.at[k] if g < 2 else r_recv.at[k - 2, c]
 
     def contract(g, k, t, chunks=(0, CHUNKS)):
         base = own_base + t * (mate_base - own_base)
@@ -236,14 +275,14 @@
         return dot(mixers[k, 0], ret[k, c]) + dot(mixers[k, 1], ret[k, c])
 
     def await_far(g, t, c):
-        k = 2 * g + t
+        k = 2 * g - 2 + t
         part = ret.at[k, c] if t else ret.at[k, c, pl.ds(cap, rows - cap)]
         await_bytes(part, came(g, k, c))
 
     x_copy.wait()
     squares = jnp.zeros((tokens, 1), jnp.float32)
     for c in every:
-        xs = x_ref[:, c * cw : (c + 1) * cw].astype(jnp.float32)
+        xs = out_ref[:, c * cw : (c + 1) * cw].astype(jnp.float32)
         squares = squares + jnp.sum(xs * xs, axis=-1, keepdims=True)
     scale = lax.rsqrt(squares / width + EPSILON)
     partner = far * inner + mate * outer
@@ -296,7 +335,7 @@
         pick(g, 0, c)
 
     def forward_copy(g, c):
-        k = 2 * g + 1
+        k = 2 * g - 1
         return remote(
             ret.at[k, c], ret.at[k, c], f_send.at[g - 2], came(g, k, c), {"ep": mate}
         )
@@ -304,18 +343,18 @@
     def forward(g, chunks):
         @pl.loop(*chunks)
         def _(c):
-            k = 2 * g + 1
+            k = 2 * g - 1
             await_bytes(ret.at[k, c, pl.ds(cap, rows - cap)], came(g, k, c))
             forward_copy(g, c).start()
 
     def share(g, c):
         await_far(g, 0, c)
         await_far(g, 1, c)
-        fp_send[g - 2, c] = (mix(2 * g, c) + mix(2 * g + 1, c)).astype(jnp.bfloat16)
+        fp_send[g - 2, c] = (mix(2 * g - 2, c) + mix(2 * g - 1, c)).astype(jnp.bfloat16)
         part_copy(g - 2, c).start()
 
     for c in every:
-        xs = x_ref[:, c * cw : (c + 1) * cw].astype(jnp.float32)
+        xs = out_ref[:, c * cw : (c + 1) * cw].astype(jnp.float32)
         held[mine, c] = (xs * scale * pre_ref[:, c * cw : (c + 1) * cw]).astype(jnp.bfloat16)
     place(mine, (0, 1))
     pl.semaphore_wait(barrier, 2 * pz - 1 + tps - 1 + inner)
@@ -400,10 +439,11 @@
 
     @on_inner
     def _():
-        accept_all(3, (CHUNKS - 2, CHUNKS))
+        accept(3, CHUNKS - 2)
+        prepare(6, 4)
+        prepare(7, 5)
+        accept(3, CHUNKS - 1)
         accept_all(2, (0, EARLY))
-        received_in_plane(1)
-        expand(1, 0)
 
     @on_outer
     def _():
@@ -416,40 +456,46 @@
         for i in range(1, tps):
             expand(0, i)
         await_down()
-        contract(0, 1, 1)
+        contract(0, 1, 1, (0, LATER))
+
+    received_part(0)
+    begin(0)
+    on_inner(lambda: accept(2, 2))
+    begin(1)
+    on_inner(lambda: accept(2, 3))
+    on_inner(await_down)
+    received_part(1)
+    for i in range(tps):
+        complete(i)
+    contract(3, 4 + outer, outer, (0, DIRECT))
+
+    @on_outer
+    def _():
+        contract(3, 5, 0, (DIRECT, CHUNKS))
         received_in_plane(1)
-        for i in range(tps):
-            expand(1, i)
-
-    received(3)
-    expand(3, 0)
-    on_inner(lambda: accept_all(2, (2, 4)))
-    expand(3, 1)
-    on_inner(await_down)
-    contract(3, 6 + outer, outer, (0, DIRECT))
-
-    @on_outer
-    def _():
-        contract(3, 7, 0, (DIRECT, CHUNKS))
+        expand(1, 0)
         forward(3, (DIRECT, LATER))
+        contract(0, 1, 1, (LATER, CHUNKS))
+        expand(1, 1)
 
     @on_inner
     def _():
         accept_all(2, (4, 6))
-        prepare(6)
-        prepare(7)
+        received_in_plane(1)
+        expand(1, 0)
         accept(2, 6)
         share(3, 0)
+        expand(1, 1, 0, fh // TILE // 2)
         accept(2, 7)
+        expand(1, 1, fh // TILE // 2, fh // TILE // 2)
         share(3, 1)
-        expand(1, 1)
-        contract(1, 3, 1, (0, 4))
+        contract(1, 1, 1, (0, 4))
         share(3, 2)
-        contract(3, 6, 0, (DIRECT, CHUNKS))
+        contract(3, 4, 0, (DIRECT, CHUNKS))
         share(3, 3)
-        contract(1, 3, 1, (4, CHUNKS))
-        prepare(4)
-        prepare(5)
+        contract(1, 1, 1, (4, CHUNKS))
+        prepare(4, 2)
+        prepare(5, 3)
 
     received(2)
     expand(2, 0)
@@ -457,12 +503,13 @@
     on_outer(lambda: forward(3, (LATER, CHUNKS)))
     expand(2, 1)
     on_inner(lambda: share_all(3, (6, CHUNKS)))
-    contract(2, 4 + outer, 0)
+    contract(2, 2 + outer, outer, (0, PAIR))
+    contract(2, 2 + outer, 0, (PAIR, CHUNKS))
 
     @on_outer
     def _():
-        forward(2, (0, CHUNKS))
-        contract(1, 2, 0)
+        forward(2, (PAIR, CHUNKS))
+        contract(1, 0, 0)
 
 
     @on_inner
@@ -479,21 +526,26 @@
             share(2, c)
             pl.when(c < CHUNKS - 2)(lambda: pass_on(c + 2))
 
-    prepare(2 * mine)
-    prepare(2 * mine + 1)
-    await_bytes(ret.at[2 * mine, :, pl.ds(cap, rows - cap)], r_near.at[2 * mine])
-    await_bytes(ret.at[2 * mine + 1], r_near.at[2 * mine + 1])
+    def mixed(c):
+        per = fh // cw
+        at = pl.ds(pl.multiple_of(lax.rem(c, per) * cw, cw), cw)
+        return acc.at[c // per, pl.ds(0, tokens), at]
+
+    prepare(2 * mine, 0)
+    prepare(2 * mine + 1, 1)
+    await_bytes(ret.at[0, :, pl.ds(cap, rows - cap)], r_near.at[0])
+    await_bytes(ret.at[1], r_near.at[1])
 
     @pl.loop(0, CHUNKS)
     def _(c):
-        mixed[c] = mix(2 * mine, c) + mix(2 * mine + 1, c)
+        mixed(c)[...] = mix(0, c) + mix(1, c)
 
     meta_copy(0).wait_send()
     on_inner(meta_copy(1).wait_send)
     others = pl.ds(cap, rows - cap)
 
     def picked(g):
-        await_bytes(send.at[2 * g, :, others], d_send.at[2 * g])
+        await_bytes(send.at[sent(g, 0), :, others], d_send.at[sent(g, 0)])
 
     def in_plane(g):
         await_bytes(recv.at[g, :, others], r_send.at[g])
@@ -511,7 +563,7 @@
             in_plane(g)
         await_bytes(recv.at[1], r_send.at[1])
         for g in (0, 2, 3):
-            await_bytes(send.at[2 * g + 1], d_send.at[2 * g + 1])
+            await_bytes(send.at[sent(g, 1)], d_send.at[sent(g, 1)])
         for kind in range(2):
             await_bytes(fp_send.at[kind], q_send.at[kind])
 
@@ -519,35 +571,24 @@
     def _():
         await_bytes(held.at[1], n_send.at[0])
         await_bytes(recv.at[0], r_send.at[0])
-        in_plane(2)
-        await_bytes(ret.at[5], f_send.at[0])
-        some = pl.ds(DIRECT, CHUNKS - DIRECT)
-        await_bytes(recv.at[3, pl.ds(0, DIRECT)], r_send.at[3])
-        await_bytes(recv.at[3, some, others], r_send.at[3])
-        await_bytes(ret.at[7, some], f_send.at[1])
-
-    def out_copy(b):
-        at = pl.ds(b * (tokens // BLOCKS), tokens // BLOCKS)
-        return pltpu.make_async_copy(x_ref.at[at], out_hbm.at[at], o_sem.at[b])
+        for g, direct in ((2, PAIR), (3, DIRECT)):
+            some = pl.ds(direct, CHUNKS - direct)
+            await_bytes(recv.at[g, pl.ds(0, direct)], r_send.at[g])
+            await_bytes(recv.at[g, some, others], r_send.at[g])
+            await_bytes(ret.at[2 * g - 1, some], f_send.at[g - 2])
 
     squares = jnp.zeros((tokens, 1), jnp.float32)
     for c in every:
         await_part(mine, c)
-        total = mixed[c] + fp_recv[mine, c].astype(jnp.float32)
-        mixed[c] = total
+        total = mixed(c)[...] + fp_recv[mine, c].astype(jnp.float32)
+        mixed(c)[...] = total
         squares = squares + jnp.sum(total * total, axis=-1, keepdims=True)
     scale = lax.rsqrt(squares / width + EPSILON)
-    for b in range(BLOCKS):
-        own = slice(b * (tokens // BLOCKS), (b + 1) * (tokens // BLOCKS))
-        for c in every:
-            at = slice(c * cw, (c + 1) * cw)
-            x_ref[own, at] = (mixed[c, own] * scale[own] * post_ref[:, at]).astype(jnp.bfloat16)
-        out_copy(b).start()
+    for c in every:
+        at = slice(c * cw, (c + 1) * cw)
+        out_ref[:, at] = (mixed(c)[...] * scale * post_ref[:, at]).astype(jnp.bfloat16)
 
     on_inner(lambda: await_bytes(fp_recv.at[1], q_send.at[2]))
-
-    for b in range(BLOCKS):
-        out_copy(b).wait()
 
 
 def local(inputs, pre_gain, expert_ids, route_weights, gate_proj, up_proj, down_proj, post_gain):
@@ -562,36 +603,35 @@
     fh = gate_proj.shape[2]
     bf16, f32 = jnp.bfloat16, jnp.float32
     vmem = pl.BlockSpec(memory_space=pltpu.VMEM)
-    hbm = pl.BlockSpec(memory_space=pl.ANY)
+    hbm = pl.BlockSpec(memory_space=pltpu.HBM)
     dma = pltpu.SemaphoreType.DMA
     return pl.pallas_call(
         functools.partial(kernel, n, tps, cap),
-        out_shape=jax.ShapeDtypeStruct((tokens, width), bf16),
+        out_shape=pltpu.VMEM((tokens, width), bf16),
         in_specs=[hbm, vmem, vmem, vmem, hbm, hbm, hbm, vmem],
-        out_specs=hbm,
+        out_specs=vmem,
         scratch_shapes=[
-            pltpu.VMEM((tokens, width), bf16),
             pltpu.VMEM((tps, width, fh), bf16),
             pltpu.VMEM((tps, width, fh), bf16),
             pltpu.VMEM((tps, fh, width), bf16),
             pltpu.VMEM((4, CHUNKS, tokens, cw), bf16),
             pltpu.VMEM((4, 8, tokens), f32),
-            pltpu.VMEM((8, CHUNKS, rows, cw), bf16),
+            pltpu.VMEM((7, CHUNKS, rows, cw), bf16),
             pltpu.VMEM((4, CHUNKS, rows, cw), bf16),
-            pltpu.VMEM((8, CHUNKS, rows, cw), bf16),
+            pltpu.VMEM((6, CHUNKS, rows, cw), bf16),
             pltpu.VMEM((2, CHUNKS, tokens, cw), bf16),
             pltpu.VMEM((2, CHUNKS, tokens, cw), bf16),
-            pltpu.VMEM((CHUNKS, tokens, cw), f32),
+            pltpu.VMEM((2 * tps, max(rows, tokens), fh), f32),
             pltpu.VMEM((4, tps, rows, fh), bf16),
             pltpu.VMEM((8, 8, tokens), f32),
-            pltpu.VMEM((8, 2, tokens, rows), bf16),
+            pltpu.VMEM((6, 2, tokens, rows), bf16),
             dma, dma((3,)), dma((3, tps - 1)), dma((3, tps - 1)),
             dma((2,)), dma((3, CHUNKS)), dma((2,)), dma((4,)),
-            dma((8,)), dma((4,)), dma((4,)), dma((4,)), dma((4, CHUNKS)),
-            dma((2,)), dma((3,)), dma((2, CHUNKS)), dma((BLOCKS,)),
+            dma((7,)), dma((5,)), dma((4,)), dma((2,)), dma((4, CHUNKS)),
+            dma((2,)), dma((3,)), dma((2, CHUNKS)),
         ],
         compiler_params=pltpu.CompilerParams(
-            collective_id=0, has_side_effects=True, vmem_limit_bytes=67043328
+            collective_id=0, has_side_effects=True, vmem_limit_bytes=67043328 - 2**20
         ),
     )(
         inputs, pre_gain[None, :], expert_ids.T, route_weights.T,

time: 104 us -> 99.8 us (0.960); the launches traced: 104 us -> 98.7 us
  Pallas kernels: 102 us -> 97.7 us
  local copies, waits for them, and re-layouts: 2.3 us -> 0.97 us
    pallas_call x1, Pallas kernels: 102 us -> 97.7 us  [local(): pl.pallas_call(functools.partial(kernel, n, tps, cap), out_shape=pltpu.VM...]
    unnamed x1, local copies, waits for them, and re-layouts: 2.3 us -> 0.97 us
where the time goes in v4:
time: 99.8 us; the launch traced here: 98.7 us
  Pallas kernels  97.7 us (98%)
    pallas_call x1, Pallas kernels, local(): pl.pallas_call(functools.partial(kernel, n, tps, cap), out_shape=pltpu.VM...  97.7 us

profile of v4, /device:TPU:8, one launch (start us, length us, event | category | flops | bytes accessed | tf_op | source)
XLA Modules:
  0.0 98.7 jit_solution(15525004780143945481)
XLA Ops:
  0.0 97.7 %shard_map.82 = bf16[256,2048]{1,0:T(8,128)(2,1)S(1)} custom-call(bf16[256,2048]{1,0:T(8,128)(2,1)} %x_hbm.1, f32[1,2048]{1,0:T(1,128)} %bitcast.4, s32[2,256]{1,0:T(2,128)} %bitcast.6, f32[2,256]{1,0:T(2,128)} %bitcast.7, bf16[1,2048,1024]{2,1,0:T(8,128)(2,1)} %gate_ref.1, bf16[1,2048,1024]{2,1,0:T(8,128)(2,1)} %up_ref.1, bf16[1,1024,2048]{2,1,0:T(8,128)(2,1)} %down_ref.1, ...), custom_call_target="tpu_custom_call" | custom-call | tf_op jit(solution)/shard_map/pallas_call | solution.py:608
  97.7 1.0 copy.10

commit v5 on v4

--- a/solution.py
+++ b/solution.py
@@ -14,6 +14,7 @@
 DIRECT = 4
 EARLY = 2
 SPLIT = 6
+STRAIGHT = 6
 LATER = 6
 BLOCKS = 4
 PAIR = 2
@@ -34,10 +35,10 @@
 
 def kernel(
     n, tps, cap,
-    x_hbm, pre_ref, ids_ref, route_ref, gate_ref, up_ref, down_ref, post_ref, out_ref,
-    gate_v, up_v, down_v, held, meta, send, recv, ret,
+    x_hbm, pre_hbm, ids_hbm, route_hbm, gate_ref, up_ref, down_ref, post_hbm, out_ref,
+    pre_ref, ids_ref, route_ref, post_ref, gate_v, up_v, down_v, held, meta, send, recv, ret,
     fp_send, fp_recv, acc, hidden, places, mixers,
-    x_sem, w_local, w_send, w_recv, n_send, n_recv, m_send, m_recv,
+    x_sem, s_sem, w_local, w_send, w_recv, n_send, n_recv, m_send, m_recv,
     d_send, d_recv, r_send, r_near, r_recv, f_send, q_send, q_recv,
 ):
     tokens, width = out_ref.shape
@@ -72,14 +73,19 @@
 
     x_copy = pltpu.make_async_copy(x_hbm, out_ref, x_sem)
     x_copy.start()
+    small_copies = [
+        pltpu.make_async_copy(src, dst, s_sem.at[i])
+        for i, (src, dst) in enumerate(
+            ((pre_hbm, pre_ref), (ids_hbm, ids_ref), (route_hbm, route_ref), (post_hbm, post_ref))
+        )
+    ]
+    for copy in small_copies:
+        copy.start()
     weights = ((gate_ref, gate_v), (up_ref, up_v), (down_ref, down_v))
     local_copies = [
         pltpu.make_async_copy(src.at[0], dst.at[core], w_local.at[w])
         for w, (src, dst) in enumerate(weights)
     ]
-    for copy in local_copies:
-        copy.start()
-
     barrier = pltpu.get_barrier_semaphore()
 
     @pl.loop(1, pz)
@@ -116,10 +122,6 @@
         ]
         for w, (src, dst) in enumerate(weights)
     ]
-    meta[mine, 0:2, :] = ids_ref[...].astype(jnp.float32)
-    meta[mine, 2:4, :] = route_ref[...]
-    meta[mine, 4:8, :] = jnp.zeros((4, tokens), jnp.float32)
-
     def place(g, ts):
         values = meta[g]
         experts_col = lax.broadcasted_iota(jnp.int32, (n, 1), 0).astype(jnp.float32)
@@ -240,7 +242,7 @@
             hidden[g, h, :, at] = activate(gate, up)
 
     def came(g, k, c):
-        return r_near.at[k] if g < 2 else r_recv.at[k - 2, c]
+        return r_near.at[min(k, 2)] if g < 2 else r_recv.at[k - 2, c]
 
     def contract(g, k, t, chunks=(0, CHUNKS)):
         base = own_base + t * (mate_base - own_base)
@@ -279,6 +281,8 @@
         part = ret.at[k, c] if t else ret.at[k, c, pl.ds(cap, rows - cap)]
         await_bytes(part, came(g, k, c))
 
+    for copy in small_copies:
+        copy.wait()
     x_copy.wait()
     squares = jnp.zeros((tokens, 1), jnp.float32)
     for c in every:
@@ -353,24 +357,35 @@
         fp_send[g - 2, c] = (mix(2 * g - 2, c) + mix(2 * g - 1, c)).astype(jnp.bfloat16)
         part_copy(g - 2, c).start()
 
-    for c in every:
-        xs = out_ref[:, c * cw : (c + 1) * cw].astype(jnp.float32)
-        held[mine, c] = (xs * scale * pre_ref[:, c * cw : (c + 1) * cw]).astype(jnp.bfloat16)
-    place(mine, (0, 1))
-    pl.semaphore_wait(barrier, 2 * pz - 1 + tps - 1 + inner)
     def await_peers(w):
         for copy in peer_copies[w]:
             copy.wait()
 
+    def normalise(chunks):
+        for c in chunks:
+            xs = out_ref[:, c * cw : (c + 1) * cw].astype(jnp.float32)
+            held[mine, c] = (xs * scale * pre_ref[:, c * cw : (c + 1) * cw]).astype(jnp.bfloat16)
+
+    normalise(range(EARLY))
+    meta[mine, 0:2, :] = ids_ref[...].astype(jnp.float32)
+    meta[mine, 2:4, :] = route_ref[...]
+    meta[mine, 4:8, :] = jnp.zeros((4, tokens), jnp.float32)
+    pl.semaphore_wait(barrier, 2 * pz - 1 + tps - 1 + inner)
     meta_copy(0).start()
-
-    @pl.loop(0, outer * CHUNKS + inner * EARLY)
-    def _(c):
+    for c in range(EARLY):
         rows_copy(0, c).start()
-
-    for copies in peer_copies:
+    normalise(range(EARLY, CHUNKS))
+
+    @on_outer
+    def _():
+        for c in range(EARLY, CHUNKS):
+            rows_copy(0, c).start()
+
+    for copies in [local_copies] + peer_copies:
         for copy in copies:
             copy.start()
+
+    place(mine, (0, 1))
 
     @pl.loop(0, CHUNKS)
     def _(c):
@@ -390,7 +405,9 @@
         await_meta(3)
         place(3, (0, 1))
         accept(3, 0)
+        prepare(6, 4)
         relay(3)
+        prepare(7, 5)
         accept(3, 1)
         received_in_plane(0)
         local_copies[0].wait()
@@ -431,6 +448,12 @@
 
     def pass_on(c):
         await_part(1, c)
+
+        @pl.when(c >= STRAIGHT)
+        def _():
+            value = fp_recv[1, c].astype(jnp.float32) + mix(6, c)
+            fp_recv[1, c] = value.astype(jnp.bfloat16)
+
         part_copy(2, c).start()
 
     def await_down():
@@ -440,8 +463,8 @@
     @on_inner
     def _():
         accept(3, CHUNKS - 2)
-        prepare(6, 4)
-        prepare(7, 5)
+        received_in_plane(1)
+        expand(1, 0, 0, fh // TILE // 2)
         accept(3, CHUNKS - 1)
         accept_all(2, (0, EARLY))
 
@@ -481,8 +504,7 @@
     @on_inner
     def _():
         accept_all(2, (4, 6))
-        received_in_plane(1)
-        expand(1, 0)
+        expand(1, 0, fh // TILE // 2, fh // TILE // 2)
         accept(2, 6)
         share(3, 0)
         expand(1, 1, 0, fh // TILE // 2)
@@ -493,7 +515,9 @@
         share(3, 2)
         contract(3, 4, 0, (DIRECT, CHUNKS))
         share(3, 3)
-        contract(1, 1, 1, (4, CHUNKS))
+        contract(1, 1, 1, (4, STRAIGHT))
+        contract(1, 6, 0, (STRAIGHT, CHUNKS))
+        prepare(2, 6)
         prepare(4, 2)
         prepare(5, 3)
 
@@ -520,6 +544,8 @@
 
         share_all(2, (0, 2))
         contract(0, 0, 0)
+        some = pl.ds(STRAIGHT, CHUNKS - STRAIGHT)
+        await_bytes(ret.at[6, some, pl.ds(cap, rows - cap)], r_near.at[2])
 
         @pl.loop(2, CHUNKS)
         def _(c):
@@ -534,11 +560,20 @@
     prepare(2 * mine, 0)
     prepare(2 * mine + 1, 1)
     await_bytes(ret.at[0, :, pl.ds(cap, rows - cap)], r_near.at[0])
-    await_bytes(ret.at[1], r_near.at[1])
-
-    @pl.loop(0, CHUNKS)
+    on_inner(lambda: await_bytes(ret.at[1], r_near.at[1]))
+    on_outer(lambda: await_bytes(ret.at[1, pl.ds(0, STRAIGHT)], r_near.at[1]))
+
+    @pl.loop(0, STRAIGHT)
     def _(c):
         mixed(c)[...] = mix(0, c) + mix(1, c)
+
+    @pl.loop(STRAIGHT, CHUNKS)
+    def _(c):
+        mixed(c)[...] = mix(0, c)
+
+        @on_inner
+        def _():
+            mixed(c)[...] = mixed(c)[...] + mix(1, c)
 
     meta_copy(0).wait_send()
     on_inner(meta_copy(1).wait_send)
@@ -561,7 +596,9 @@
             picked(g)
         for g in (2, 3):
             in_plane(g)
-        await_bytes(recv.at[1], r_send.at[1])
+        some = pl.ds(STRAIGHT, CHUNKS - STRAIGHT)
+        await_bytes(recv.at[1, pl.ds(0, STRAIGHT)], r_send.at[1])
+        await_bytes(recv.at[1, some, others], r_send.at[1])
         for g in (0, 2, 3):
             await_bytes(send.at[sent(g, 1)], d_send.at[sent(g, 1)])
         for kind in range(2):
@@ -608,9 +645,13 @@
     return pl.pallas_call(
         functools.partial(kernel, n, tps, cap),
         out_shape=pltpu.VMEM((tokens, width), bf16),
-        in_specs=[hbm, vmem, vmem, vmem, hbm, hbm, hbm, vmem],
+        in_specs=[hbm] * 8,
         out_specs=vmem,
         scratch_shapes=[
+            pltpu.VMEM((1, width), f32),
+            pltpu.VMEM((choices, tokens), jnp.int32),
+            pltpu.VMEM((choices, tokens), f32),
+            pltpu.VMEM((1, width), f32),
             pltpu.VMEM((tps, width, fh), bf16),
             pltpu.VMEM((tps, width, fh), bf16),
             pltpu.VMEM((tps, fh, width), bf16),
@@ -618,16 +659,16 @@
             pltpu.VMEM((4, 8, tokens), f32),
             pltpu.VMEM((7, CHUNKS, rows, cw), bf16),
             pltpu.VMEM((4, CHUNKS, rows, cw), bf16),
-            pltpu.VMEM((6, CHUNKS, rows, cw), bf16),
+            pltpu.VMEM((7, CHUNKS, rows, cw), bf16),
             pltpu.VMEM((2, CHUNKS, tokens, cw), bf16),
             pltpu.VMEM((2, CHUNKS, tokens, cw), bf16),
             pltpu.VMEM((2 * tps, max(rows, tokens), fh), f32),
             pltpu.VMEM((4, tps, rows, fh), bf16),
             pltpu.VMEM((8, 8, tokens), f32),
-            pltpu.VMEM((6, 2, tokens, rows), bf16),
-            dma, dma((3,)), dma((3, tps - 1)), dma((3, tps - 1)),
+            pltpu.VMEM((7, 2, tokens, rows), bf16),
+            dma, dma((4,)), dma((3,)), dma((3, tps - 1)), dma((3, tps - 1)),
             dma((2,)), dma((3, CHUNKS)), dma((2,)), dma((4,)),
-            dma((7,)), dma((5,)), dma((4,)), dma((2,)), dma((4, CHUNKS)),
+            dma((7,)), dma((5,)), dma((4,)), dma((3,)), dma((4, CHUNKS)),
             dma((2,)), dma((3,)), dma((2, CHUNKS)),
         ],
         compiler_params=pltpu.CompilerParams(

time: 99.8 us -> 98.3 us (0.985)
  no operation moved by 1% of the time
where the time goes in v5:
time: 98.3 us; the launch traced here: 98 us
  Pallas kernels  97.1 us (99%)
    pallas_call x1, Pallas kernels, local(): pl.pallas_call(functools.partial(kernel, n, tps, cap), out_shape=pltpu.VM...  97.1 us

profile of v5, /device:TPU:8, one launch (start us, length us, event | category | flops | bytes accessed | tf_op | source)
XLA Modules:
  0.0 98.0 jit_solution(15777046791517102539)
XLA Ops:
  0.0 97.1 %shard_map.82 = bf16[256,2048]{1,0:T(8,128)(2,1)S(1)} custom-call(bf16[256,2048]{1,0:T(8,128)(2,1)} %x_hbm.1, f32[1,2048]{1,0:T(1,128)} %bitcast.4, s32[2,256]{1,0:T(2,128)} %bitcast.6, f32[2,256]{1,0:T(2,128)} %bitcast.7, bf16[1,2048,1024]{2,1,0:T(8,128)(2,1)} %gate_ref.1, bf16[1,2048,1024]{2,1,0:T(8,128)(2,1)} %up_ref.1, bf16[1,1024,2048]{2,1,0:T(8,128)(2,1)} %down_ref.1, ...), custom_call_target="tpu_custom_call" | custom-call | tf_op jit(solution)/shard_map/pallas_call | solution.py:645
  97.1 1.0 copy.10

commit v6 on v5

--- a/solution.py
+++ b/solution.py
@@ -389,8 +389,8 @@
 
     @pl.loop(0, CHUNKS)
     def _(c):
+        on_inner(lambda: pick(0, 1, c))
         pick(mine, 0, c)
-        on_inner(lambda: pick(0, 1, c))
 
     @on_inner
     def _():

time: 98.3 us -> 98.2 us (level)
  no operation moved by 1% of the time
where the time goes in v6:
time: 98.2 us; the launch traced here: 98 us
  Pallas kernels  97 us (99%)
    pallas_call x1, Pallas kernels, local(): pl.pallas_call(functools.partial(kernel, n, tps, cap), out_shape=pltpu.VM...  97 us

profile of v6, /device:TPU:8, one launch (start us, length us, event | category | flops | bytes accessed | tf_op | source)
XLA Modules:
  0.0 98.0 jit_solution(3731726641430166378)
XLA Ops:
  0.0 97.0 %shard_map.82 = bf16[256,2048]{1,0:T(8,128)(2,1)S(1)} custom-call(bf16[256,2048]{1,0:T(8,128)(2,1)} %x_hbm.1, f32[1,2048]{1,0:T(1,128)} %bitcast.4, s32[2,256]{1,0:T(2,128)} %bitcast.6, f32[2,256]{1,0:T(2,128)} %bitcast.7, bf16[1,2048,1024]{2,1,0:T(8,128)(2,1)} %gate_ref.1, bf16[1,2048,1024]{2,1,0:T(8,128)(2,1)} %up_ref.1, bf16[1,1024,2048]{2,1,0:T(8,128)(2,1)} %down_ref.1, ...), custom_call_target="tpu_custom_call" | custom-call | tf_op jit(solution)/shard_map/pallas_call | solution.py:645
  97.0 1.0 copy.10
